TPU v7x, 32 devices: a whole 2x2x4 slice. The times are simulated.
32 devices in a mesh: sp: 4 (over y, x), dp: 8 (over z, core).
Axes of the slice: x: 2, y: 2, z: 4, core: 2. Of those that a mesh axis runs over, the one named last changes fastest.
Arguments:
- tokens: bfloat16 [8, 768, 4096], P('dp', 'sp'), may hold values from -30 to 30
- query_weight: bfloat16 [4096, 512], P('dp', 'sp'), may hold values from -0.09375 to 0.09375
- key_weight: bfloat16 [4096, 512], P('dp', 'sp'), may hold values from -0.09375 to 0.09375
- value_weight: bfloat16 [4096, 512], P('dp', 'sp'), may hold values from -0.09375 to 0.09375
- cum_gate: float32 [8, 4, 768], P('dp', 'sp'), may hold values from -3072 to 0, as said below
Outputs:
- attended: bfloat16 [8, 768, 512], P('dp', 'sp')
Inputs may be any that keep to these rules, and one draw needn't show every extreme that they name: `cum_gate`: never rising along positions; the first position holds one step's log gate.
All inputs are finite; a program needn't handle non-finite values.
Results may differ from a plain program's by a relative error of at most 0.0076.
The roundings to bfloat16 on the way count: a program that leaves them out, or rounds other values in their place, can miss the bound.
Values may be sent and summed in bfloat16 or wider, within the bound.
No kernel may reach another device: no remote copies, remote signals or barrier semaphores. Data moves between devices by JAX's collectives and lax.ppermute only.
A program may use at most 128 MiB of HBM per device.

v0:
```python
import jax
import jax.numpy as jnp
from jax import lax
from jax.sharding import PartitionSpec as P

block_rows = 512


def attend(queries, keys, values, gates):
    length = queries.shape[0]
    scale = queries.shape[1] ** (-0.5)
    pieces = []
    for start in range(0, length, block_rows):
        finish = min(start + block_rows, length)
        scores = (
            jnp.dot(queries[start:finish], keys[:finish].T, preferred_element_type=jnp.float32)
            * scale
        )
        scores = scores + gates[start:finish, None] - gates[None, :finish]
        rows_at = start + lax.broadcasted_iota(jnp.int32, scores.shape, 0)
        cols_at = lax.broadcasted_iota(jnp.int32, scores.shape, 1)
        scores = jnp.where(cols_at <= rows_at, scores, -1e30)
        top = jnp.max(scores, axis=1, keepdims=True)
        weights = jnp.exp(scores - top)
        total = jnp.sum(weights, axis=1, keepdims=True)
        summed = jnp.dot(
            weights.astype(jnp.bfloat16), values[:finish], preferred_element_type=jnp.float32
        )
        pieces.append((summed / total).astype(jnp.bfloat16))
    return jnp.concatenate(pieces, axis=0)


def body(tokens, query_weight, key_weight, value_weight, cum_gate):
    width = query_weight.shape[1]
    full_query, full_key, full_value = (
        lax.all_gather(query_weight, "dp", axis=0, tiled=True),
        lax.all_gather(key_weight, "dp", axis=0, tiled=True),
        lax.all_gather(value_weight, "dp", axis=0, tiled=True),
    )
    stacked = jnp.concatenate([full_query, full_key, full_value], axis=1)
    own_rows = tokens[0]
    projected = jnp.dot(
        lax.all_gather(own_rows, "sp", axis=0, tiled=True),
        stacked,
        preferred_element_type=jnp.float32,
    )
    queries = projected[:, :width].astype(jnp.bfloat16)
    keys = projected[:, width : 2 * width].astype(jnp.bfloat16)
    values = projected[:, 2 * width :].astype(jnp.bfloat16)
    head_out = attend(queries, keys, values, cum_gate[0, 0])
    gathered = lax.all_to_all(head_out, "sp", split_axis=0, concat_axis=1, tiled=True)
    return gathered[None]


def solution(mesh):
    in_specs = (
        P("dp", "sp", None),
        P("dp", "sp"),
        P("dp", "sp"),
        P("dp", "sp"),
        P("dp", "sp", None),
    )
    out_specs = P("dp", "sp", None)
    return jax.shard_map(body, mesh=mesh, in_specs=in_specs, out_specs=out_specs, check_vma=False)
```

profile of v0, /device:TPU:0, one launch (start us, length us, event | category | flops | bytes accessed | tf_op | source)
XLA Modules:
  0.0 176.3 jit_solution(13971013935284889980)
XLA Ops:
  6.5 0.0 all-gather.6.cloned.1.call-start
  6.5 0.7 all-gather.6.cloned.1.call-update
  7.3 0.0 all-gather.8.cloned.1.call-start
  7.3 0.7 all-gather.8.cloned.1.call-update
  8.0 0.0 all-gather.10.cloned.1.call-start
  8.1 0.7 all-gather.10.cloned.1.call-update
  8.7 0.0 all-gather.12.cloned.1.call-start
  8.8 0.5 all-gather.12.cloned.1.call-update
  9.3 0.7 reduce
  10.0 0.0 slice-start
  10.0 0.0 slice-start.1
  10.1 23.9 %all-gather.6.cloned.1.call-done = bf16[4096,128]{1,0:T(8,128)(2,1)} async-done(((bf16[512,128]{1,0:T(8,128)(2,1)}), bf16[4096,128]{1,0:T(8,128)(2,1)}) %all-gather.6.cloned.1.call-update) | async-done | bytes 1048592 | tf_op jit(solution)/shard_map/all_gather | solution.py:36
  33.9 23.5 %all-gather.8.cloned.1.call-done = bf16[4096,128]{1,0:T(8,128)(2,1)} async-done(((bf16[512,128]{1,0:T(8,128)(2,1)}), bf16[4096,128]{1,0:T(8,128)(2,1)}) %all-gather.8.cloned.1.call-update) | async-done | bytes 1048592 | tf_op jit(solution)/shard_map/all_gather | solution.py:37
  57.4 23.5 %all-gather.10.cloned.1.call-done = bf16[4096,128]{1,0:T(8,128)(2,1)} async-done(((bf16[512,128]{1,0:T(8,128)(2,1)}), bf16[4096,128]{1,0:T(8,128)(2,1)}) %all-gather.10.cloned.1.call-update) | async-done | bytes 1048592 | tf_op jit(solution)/shard_map/all_gather | solution.py:38
  80.9 71.4 %all-gather.12.cloned.1.call-done = bf16[1,768,4096]{2,1,0:T(8,128)(2,1)} async-done(((bf16[1,192,4096]{2,1,0:T(8,128)(2,1)}), bf16[1,768,4096]{2,1,0:T(8,128)(2,1)}) %all-gather.12.cloned.1.call-update) | async-done | bytes 6291472 | tf_op jit(solution)/shard_map/all_gather | solution.py:43
  152.3 6.4 %fusion.18 = bf16[768,384]{0,1:T(8,128)(2,1)S(1)} fusion(bf16[1,768,4096]{2,1,0:T(8,128)(2,1)} %all-gather.12.cloned.1.call-done, bf16[4096,128]{1,0:T(8,128)(2,1)} %all-gather.10.cloned.1.call-done, bf16[4096,128]{1,0:T(8,128)(2,1)} %all-gather.8.cloned.1.call-done, bf16[4096,128]{1,0:T(8,128)(2,1)} %all-gather.6.cloned.1.call-done), kind=kOutput, calls=%fused_computation.16 | convolution fusion | flops 2425651200 | bytes 10027008 | tf_op jit(solution)/shard_map/dot_general | solution.py:42
  158.7 0.0 slice-done
  158.7 0.4 fusion.40
  159.1 0.3 fusion.27
  159.4 0.3 fusion.24
  159.7 0.0 slice-done.1
  159.8 0.4 fusion.41
  160.1 0.2 fusion.25
  160.3 0.4 fusion.23
  160.7 8.1 %all_to_all.16 = bf16[4,192,128]{2,1,0:T(8,128)(2,1)S(1)} all-to-all(bf16[4,192,128]{2,1,0:T(8,128)(2,1)S(1)} %bitcast.13), channel_id=1, replica_groups=mesh['sp'=4,'dp'=8] {'sp'}, dimensions={0} | all-to-all | bytes 393216 | tf_op jit(solution)/shard_map/all_to_all | solution.py:51
  168.8 0.2 copy.6
  169.0 0.8 broadcast_in_dim.20
  (2 shorter events, 0.0 us)
Async XLA Ops:
  6.5 27.4 %all-gather.6.cloned.1.call-start = ((), (), s32[]{:S(2)}) async-start(), calls=%async_computation.1 | async-start | bytes 1179648 | tf_op jit(solution)/shard_map/all_gather | solution.py:36
  7.3 50.1 %all-gather.8.cloned.1.call-start = ((), (), s32[]{:S(2)}) async-start(), calls=%async_computation.2 | async-start | bytes 1179648 | tf_op jit(solution)/shard_map/all_gather | solution.py:37
  8.0 72.9 %all-gather.10.cloned.1.call-start = ((), (), s32[]{:S(2)}) async-start(), calls=%async_computation.3 | async-start | bytes 1179648 | tf_op jit(solution)/shard_map/all_gather | solution.py:38
  8.7 143.5 %all-gather.12.cloned.1.call-start = ((), (), s32[]{:S(2)}) async-start(), calls=%async_computation.4 | async-start | bytes 7864320 | tf_op jit(solution)/shard_map/all_gather | solution.py:43
  10.0 148.6 %slice-start = ((f32[1,1,768]{2,1,0:T(1,128)}), f32[1,1,256]{2,1,0:T(1,128)S(1)}, s32[]{:S(2)}) async-start(f32[1,1,768]{2,1,0:T(1,128)} %param.9), calls=%async_computation.5 | async-start | bytes 2048 | tf_op jit(solution)/shard_map/slice | solution.py:19
  10.0 149.7 %slice-start.1 = ((f32[1,1,768]{2,1,0:T(1,128)}), f32[1,1,512]{2,1,0:T(1,128)S(1)}, s32[]{:S(2)}) async-start(f32[1,1,768]{2,1,0:T(1,128)} %param.9), calls=%async_computation.6 | async-start | bytes 4096 | tf_op jit(solution)/shard_map/slice | solution.py:19
Sparse Core Ops, SparseCore 0:
  8.9 24.9 all-gather.5
  35.5 21.8 all-gather.7
  59.0 21.8 all-gather.9
  82.6 69.6 all-gather.11
where the time goes:
time: 176 us
  waiting for transfers between devices  145 us (82%)
  between operations  13.2 us (8%)
  blocking collectives  8.09 us (5%)
  matrix products  7.93 us (5%)
    all_gather x1, waiting for transfers between devices, body(): lax.all_gather(own_rows, 'sp', axis=0, tiled=True)  71.4 us
    all_gather x1, waiting for transfers between devices, body(): lax.all_gather(query_weight, 'dp', axis=0, tiled=True)  23.9 us
    all_gather x1, waiting for transfers between devices, body(): lax.all_gather(value_weight, 'dp', axis=0, tiled=True)  23.5 us
    all_gather x1, waiting for transfers between devices, body(): lax.all_gather(key_weight, 'dp', axis=0, tiled=True)  23.5 us
    all_to_all x1, blocking collectives, body(): lax.all_to_all(head_out, 'sp', split_axis=0, concat_axis=1, tiled=True)  8.09 us
    dot_general x1, matrix products, body(): jnp.dot(lax.all_gather(own_rows, 'sp', axis=0, tiled=True), stacked, pref...  6.41 us
  transfers between devices with their start and end apart: 4, of which 4 were waited for; matrix products, arithmetic and copies ran while one was open for 0% of the time, Pallas kernels for 0%

commit v1 on v0

v1 whole, which is shorter than its diff:
```python
import math

import jax
import jax.numpy as jnp
from jax import lax
from jax.sharding import PartitionSpec as P


block_rows = 512


def attend(queries, keys, values, gates):
    length = queries.shape[0]
    scale = queries.shape[1] ** (-0.5)
    pieces = []
    for start in range(0, length, block_rows):
        finish = min(start + block_rows, length)
        scores = (
            jnp.dot(queries[start:finish], keys[:finish].T, preferred_element_type=jnp.float32)
            * scale
        )
        scores = scores + gates[start:finish, None] - gates[None, :finish]
        rows_at = start + lax.broadcasted_iota(jnp.int32, scores.shape, 0)
        cols_at = lax.broadcasted_iota(jnp.int32, scores.shape, 1)
        scores = jnp.where(cols_at <= rows_at, scores, -1e30)
        top = jnp.max(scores, axis=1, keepdims=True)
        weights = jnp.exp(scores - top)
        total = jnp.sum(weights, axis=1, keepdims=True)
        summed = jnp.dot(
            weights.astype(jnp.bfloat16), values[:finish], preferred_element_type=jnp.float32
        )
        pieces.append((summed / total).astype(jnp.bfloat16))
    return jnp.concatenate(pieces, axis=0)


def make_body(sp, dp):
    cores = 2
    planes = dp // cores
    side = math.isqrt(sp)

    def send(array, axis, count, target):
        return lax.ppermute(array, axis, [(i, target(i)) for i in range(count)])

    def shift_x(k):
        return lambda i: i // side * side + (i + k) % side

    def shift_y(k):
        return lambda i: (i // side + k) % side * side + i % side

    def shift_z(k):
        return lambda i: (i + k * cores) % dp

    def body(tokens, query_weight, key_weight, value_weight, cum_gate):
        width = query_weight.shape[1]
        own = tokens[0]
        rows = own.shape[0]
        half = rows // 2
        s = lax.axis_index("sp")
        d = lax.axis_index("dp")
        y, x = s // side, s % side
        z, core = d // cores, d % cores
        local = jnp.concatenate([query_weight, key_weight, value_weight], axis=1)
        first, second = own[:half], own[half:]

        chunks = {(0, 0): [first, second]}
        for k in range(1, side):
            late = send(second, "sp", sp, shift_x(k))
            chunks[(0, k)] = [send(first, "sp", sp, shift_x(k)), late]
            chunks[(k, 0)] = [send(first, "sp", sp, shift_y(k)), send(second, "sp", sp, shift_y(k))]
        stripes = [local]
        for k in range(1, planes):
            stripes.append(send(local, "dp", dp, shift_z(k)))
        for j in range(1, side):
            for k in range(1, side):
                early = send(chunks[(j, 0)][0], "sp", sp, shift_x(k))
                late = send(chunks[(0, k)][1], "sp", sp, shift_y(j))
                chunks[(j, k)] = [early, late]
        whole = jnp.zeros((planes, cores) + local.shape, local.dtype)
        for k in range(planes):
            stripe = stripes[k]
            twin = send(stripe, "dp", dp, lambda i: i // cores * cores + (i + 1) % cores)
            at = (z - k) % planes
            whole = lax.dynamic_update_slice(whole, stripe[None, None], (at, core, 0, 0))
            whole = lax.dynamic_update_slice(whole, twin[None, None], (at, (core + 1) % cores, 0, 0))
        stacked = whole.reshape(dp * local.shape[0], local.shape[1])

        projected = jnp.zeros((side, side, rows, 3 * width), jnp.bfloat16)
        for (j, k), parts in chunks.items():
            for n, part in enumerate(parts):
                piece = jnp.dot(part, stacked, preferred_element_type=jnp.float32)
                piece = piece.astype(jnp.bfloat16)
                at = ((y - j) % side, (x - k) % side, n * half, 0)
                projected = lax.dynamic_update_slice(projected, piece[None, None], at)
        projected = projected.reshape(sp * rows, 3 * width)
        queries = projected[:, :width]
        keys = projected[:, width : 2 * width]
        values = projected[:, 2 * width :]
        head_out = attend(queries, keys, values, cum_gate[0, 0])
        gathered = lax.all_to_all(head_out, "sp", split_axis=0, concat_axis=1, tiled=True)
        return gathered[None]

    return body


def solution(mesh):
    in_specs = (
        P("dp", "sp", None),
        P("dp", "sp"),
        P("dp", "sp"),
        P("dp", "sp"),
        P("dp", "sp", None),
    )
    out_specs = P("dp", "sp", None)
    body = make_body(mesh.shape["sp"], mesh.shape["dp"])

    return jax.shard_map(body, mesh=mesh, in_specs=in_specs, out_specs=out_specs, check_vma=False)
```

time: 176 us -> 90.2 us (0.51)
  the two profiles are of different devices: /device:TPU:0 before, /device:TPU:24 now
where the time goes in v1:
time: 90.2 us; the launch traced here: 89.9 us
  waiting for transfers between devices  55 us (61%)
  starting transfers between devices  10.9 us (12%)
  blocking collectives  8.14 us (9%)
  local copies, waits for them, and re-layouts  8.08 us (9%)
  matrix products  7.02 us (8%)
    ppermute x13, waiting for transfers between devices, send(): return lax.ppermute(array, axis, [(i, target(i)) for i in range(count)])  55 us
    ppermute x13, starting transfers between devices, send(): return lax.ppermute(array, axis, [(i, target(i)) for i in range(count)])  10.9 us
    all_to_all x1, blocking collectives, body(): lax.all_to_all(head_out, 'sp', split_axis=0, concat_axis=1, tiled=True)  8.14 us
    dot_general x8, matrix products, body(): piece = jnp.dot(part, stacked, preferred_element_type=jnp.float32)  5.51 us
    unnamed x6, local copies, waits for them, and re-layouts  1.89 us
  transfers between devices with their start and end apart: 13, of which 5 were waited for; matrix products, arithmetic and copies ran while one was open for 10% of the time, Pallas kernels for 0%

profile of v1, /device:TPU:24, one launch (start us, length us, event | category | flops | bytes accessed | tf_op | source)
XLA Modules:
  0.0 89.9 jit_solution(3993441365540149502)
XLA Ops:
  0.0 0.9 %constant_dynamic-update-slice_fusion.2 = bf16[512,384]{1,0:T(8,128)(2,1)S(1)} fusion(bf16[512,128]{1,0:T(8,128)(2,1)} %param.6), kind=kLoop, calls=%fused_computation.65 | loop fusion | bytes 262144
  0.9 0.9 %constant_dynamic-update-slice_fusion.1 = bf16[512,384]{1,0:T(8,128)(2,1)S(1)} fusion(bf16[512,384]{1,0:T(8,128)(2,1)S(1)} %constant_dynamic-update-slice_fusion.2, bf16[512,128]{1,0:T(8,128)(2,1)} %param.7), kind=kLoop, calls=%fused_computation.64 | loop fusion | bytes 262144
  1.9 0.9 %constant_dynamic-update-slice_fusion = bf16[512,384]{1,0:T(8,128)(2,1)S(1)} fusion(bf16[512,384]{1,0:T(8,128)(2,1)S(1)} %constant_dynamic-update-slice_fusion.1, bf16[512,128]{1,0:T(8,128)(2,1)} %param.8), kind=kLoop, calls=%fused_computation.63 | loop fusion | bytes 262144 | tf_op jit(solution)/shard_map/concatenate | solution.py:62
  2.8 0.1 collective-permute-start
  2.9 0.1 collective-permute-start.1
  3.0 1.9 %collective-permute-start.3 = (bf16[512,384]{1,0:T(8,128)(2,1)S(1)}, bf16[512,384]{1,0:T(8,128)(2,1)S(1)}, u32[]{:S(2)}, u32[]{:S(2)}) collective-permute-start(bf16[512,384]{1,0:T(8,128)(2,1)S(1)} %constant_dynamic-update-slice_fusion), channel_id=1, source_target_pairs={{0,4},{1,5},{2,6},{3,7},{4,0},{5,1},{6,2},{7,3},{8,12},{9,13},{10,... | collective-permute-start | bytes 1179656 | tf_op jit(solution)/shard_map/ppermute | solution.py:42
  4.9 0.4 collective-permute-start.5
  5.3 1.5 %slice_bitcast_fusion = (bf16[96,4096]{1,0:T(8,128)(2,1)S(1)}, bf16[96,4096]{1,0:T(8,128)(2,1)S(1)}) fusion(bf16[1,192,4096]{2,1,0:T(8,128)(2,1)} %param.5), kind=kLoop, calls=%fused_computation.42 | loop fusion | bytes 3145728 | tf_op jit(solution)/shard_map/slice | solution.py:63
  6.8 1.6 %collective-permute-start.8 = (bf16[96,4096]{1,0:T(8,128)(2,1)S(1)}, bf16[96,4096]{1,0:T(8,128)(2,1)S(1)}, u32[]{:S(2)}, u32[]{:S(2)}) collective-permute-start(bf16[96,4096]{1,0:T(8,128)(2,1)S(1)} %get-tuple-element.5), channel_id=1, source_target_pairs={{0,8},{8,0},{16,24},{24,16},{1,9},{9,1},{17,25},{25,17},{2,10},{10... | collective-permute-start | bytes 2359304 | tf_op jit(solution)/shard_map/ppermute | solution.py:42
  8.4 0.3 broadcast_in_dim.73
  8.7 0.1 bitcast_dynamic-update-slice_fusion.7
  8.8 1.6 %collective-permute-start.9 = (bf16[96,4096]{1,0:T(8,128)(2,1)S(1)}, bf16[96,4096]{1,0:T(8,128)(2,1)S(1)}, u32[]{:S(2)}, u32[]{:S(2)}) collective-permute-start(bf16[96,4096]{1,0:T(8,128)(2,1)S(1)} %get-tuple-element.6), channel_id=1, source_target_pairs={{0,16},{8,24},{16,0},{24,8},{1,17},{9,25},{17,1},{25,9},{2,18},{10... | collective-permute-start | bytes 2359304 | tf_op jit(solution)/shard_map/ppermute | solution.py:42
  10.4 4.3 %collective-permute-done.1 = bf16[512,384]{1,0:T(8,128)(2,1)} collective-permute-done((bf16[512,384]{1,0:T(8,128)(2,1)S(1)}, bf16[512,384]{1,0:T(8,128)(2,1)}, u32[]{:S(2)}, u32[]{:S(2)}) %collective-permute-start.1) | collective-permute-done | bytes 393248 | tf_op jit(solution)/shard_map/ppermute | solution.py:42
  14.7 1.1 %bitcast_dynamic-update-slice_fusion.6 = bf16[4,2,512,384]{3,2,1,0:T(8,128)(2,1)S(1)} fusion(bf16[4,2,512,384]{3,2,1,0:T(8,128)(2,1)S(1)} %bitcast_dynamic-update-slice_fusion.7, s32[]{:T(128)S(6)} %select_n.146, s32[]{:T(128)S(6)} %select_n.150, bf16[512,384]{1,0:T(8,128)(2,1)} %collective-permute-done), kind=kLoop, calls=%fused_computation.53 | loop fusion | bytes 786440 | tf_op jit(solution)/shard_map/dynamic_update_slice | solution.py:84
  15.8 1.1 %bitcast_dynamic-update-slice_fusion.5 = bf16[4,2,512,384]{3,2,1,0:T(8,128)(2,1)S(1)} fusion(bf16[4,2,512,384]{3,2,1,0:T(8,128)(2,1)S(1)} %bitcast_dynamic-update-slice_fusion.6, s32[]{:T(128)S(6)} %select_n.152, s32[]{:T(128)S(6)} %select_n.148, bf16[512,384]{1,0:T(8,128)(2,1)} %collective-permute-done.1), kind=kLoop, calls=%fused_computation.52 | loop fusion | bytes 786440 | tf_op jit(solution)/shard_map/dynamic_update_slice | solution.py:83
  16.8 22.8 %collective-permute-done.3 = bf16[512,384]{1,0:T(8,128)(2,1)S(1)} collective-permute-done((bf16[512,384]{1,0:T(8,128)(2,1)S(1)}, bf16[512,384]{1,0:T(8,128)(2,1)S(1)}, u32[]{:S(2)}, u32[]{:S(2)}) %collective-permute-start.3) | collective-permute-done | bytes 393248 | tf_op jit(solution)/shard_map/ppermute | solution.py:42
  39.6 1.5 %collective-permute-start.7 = (bf16[96,4096]{1,0:T(8,128)(2,1)S(1)}, bf16[96,4096]{1,0:T(8,128)(2,1)S(1)}, u32[]{:S(2)}, u32[]{:S(2)}) collective-permute-start(bf16[96,4096]{1,0:T(8,128)(2,1)S(1)} %get-tuple-element.6), channel_id=1, source_target_pairs={{0,8},{8,0},{16,24},{24,16},{1,9},{9,1},{17,25},{25,17},{2,10},{10... | collective-permute-start | bytes 2359304 | tf_op jit(solution)/shard_map/ppermute | solution.py:42
  41.1 0.1 bitcast_dynamic-update-slice_fusion.4
  41.2 0.1 bitcast_dynamic-update-slice_fusion.3
  41.2 1.6 %collective-permute-start.10 = (bf16[96,4096]{1,0:T(8,128)(2,1)S(1)}, bf16[96,4096]{1,0:T(8,128)(2,1)S(1)}, u32[]{:S(2)}, u32[]{:S(2)}) collective-permute-start(bf16[96,4096]{1,0:T(8,128)(2,1)S(1)} %get-tuple-element.5), channel_id=1, source_target_pairs={{0,16},{8,24},{16,0},{24,8},{1,17},{9,25},{17,1},{25,9},{2,18},{10... | collective-permute-start | bytes 2359304 | tf_op jit(solution)/shard_map/ppermute | solution.py:42
  42.8 0.2 collective-permute-start.6
  43.1 0.5 collective-permute-start.11
  43.6 1.4 %collective-permute-start.12 = (bf16[96,4096]{1,0:T(8,128)(2,1)S(1)}, bf16[96,4096]{1,0:T(8,128)(2,1)S(1)}, u32[]{:S(2)}, u32[]{:S(2)}) collective-permute-start(bf16[96,4096]{1,0:T(8,128)(2,1)S(1)} %collective-permute-done.8), channel_id=1, source_target_pairs={{0,16},{8,24},{16,0},{24,8},{1,17},{9,25},{17,1},{25,9},{2,18},{10... | collective-permute-start | bytes 2359304 | tf_op jit(solution)/shard_map/ppermute | solution.py:42
  45.0 0.1 bitcast_dynamic-update-slice_fusion.2
  45.1 0.1 bitcast_dynamic-update-slice_fusion.1
  45.2 0.1 bitcast_dynamic-update-slice_fusion
  45.2 0.1 broadcast_in_dim.72
  45.3 0.7 fusion.9
  46.0 0.7 fusion.11
  46.7 13.3 %collective-permute-done.7 = bf16[96,4096]{1,0:T(8,128)(2,1)S(1)} collective-permute-done((bf16[96,4096]{1,0:T(8,128)(2,1)S(1)}, bf16[96,4096]{1,0:T(8,128)(2,1)S(1)}, u32[]{:S(2)}, u32[]{:S(2)}) %collective-permute-start.7) | collective-permute-done | bytes 786464 | tf_op jit(solution)/shard_map/ppermute | solution.py:42
  60.0 0.7 fusion.13
  60.7 0.7 fusion.15
  61.4 0.7 fusion.17
  62.1 0.7 fusion.19
  62.8 12.7 %collective-permute-done.11 = bf16[96,4096]{1,0:T(8,128)(2,1)S(1)} collective-permute-done((bf16[96,4096]{1,0:T(8,128)(2,1)S(1)}, bf16[96,4096]{1,0:T(8,128)(2,1)S(1)}, u32[]{:S(2)}, u32[]{:S(2)}) %collective-permute-start.11) | collective-permute-done | bytes 786464 | tf_op jit(solution)/shard_map/ppermute | solution.py:42
  75.5 0.7 fusion.21
  76.2 2.0 %collective-permute-done.12 = bf16[96,4096]{1,0:T(8,128)(2,1)S(1)} collective-permute-done((bf16[96,4096]{1,0:T(8,128)(2,1)S(1)}, bf16[96,4096]{1,0:T(8,128)(2,1)S(1)}, u32[]{:S(2)}, u32[]{:S(2)}) %collective-permute-start.12) | collective-permute-done | bytes 786464 | tf_op jit(solution)/shard_map/ppermute | solution.py:42
  78.1 0.7 fusion.23
  78.8 0.0 slice-start.1
  78.8 0.3 fusion.39
  79.2 0.2 fusion.24
  79.4 0.4 fusion.6
  79.7 0.4 fusion.38
  80.2 0.3 fusion.26
  80.4 0.4 fusion.7
  80.9 8.1 %all_to_all.16 = bf16[4,192,128]{2,1,0:T(8,128)(2,1)S(1)} all-to-all(bf16[4,192,128]{2,1,0:T(8,128)(2,1)S(1)} %bitcast.98), channel_id=1, replica_groups=mesh['sp'=4,'dp'=8] {'sp'}, dimensions={0} | all-to-all | bytes 393216 | tf_op jit(solution)/shard_map/all_to_all | solution.py:99
  89.0 0.2 copy.6
  89.2 0.8 broadcast_in_dim.92
  (20 shorter events, 0.1 us)
Async XLA Ops:
  0.0 8.4 %copy-start.1 = (f32[1,1,768]{2,1,0:T(1,128)S(1)}, f32[1,1,768]{2,1,0:T(1,128)}, u32[]{:S(2)}) copy-start(f32[1,1,768]{2,1,0:T(1,128)} %param.9) | copy-start | bytes 9220
  2.8 6.0 %collective-permute-start = (bf16[512,384]{1,0:T(8,128)(2,1)S(1)}, bf16[512,384]{1,0:T(8,128)(2,1)}, u32[]{:S(2)}, u32[]{:S(2)}) collective-permute-start(bf16[512,384]{1,0:T(8,128)(2,1)S(1)} %constant_dynamic-update-slice_fusion), channel_id=1, source_target_pairs={{0,1},{1,0},{2,3},{3,2},{4,5},{5,4},{6,7},{7,6},{8,9},{9,8},{10,11... | collective-permute-start | bytes 1179656 | tf_op jit(solution)/shard_map/ppermute | solution.py:42
  2.9 11.8 %collective-permute-start.1 = (bf16[512,384]{1,0:T(8,128)(2,1)S(1)}, bf16[512,384]{1,0:T(8,128)(2,1)}, u32[]{:S(2)}, u32[]{:S(2)}) collective-permute-start(bf16[512,384]{1,0:T(8,128)(2,1)S(1)} %constant_dynamic-update-slice_fusion), channel_id=1, source_target_pairs={{0,2},{1,3},{2,4},{3,5},{4,6},{5,7},{6,0},{7,1},{8,10},{9,11},{10,... | collective-permute-start | bytes 1179656 | tf_op jit(solution)/shard_map/ppermute | solution.py:42
  3.0 36.6 %collective-permute-start.3 = (bf16[512,384]{1,0:T(8,128)(2,1)S(1)}, bf16[512,384]{1,0:T(8,128)(2,1)S(1)}, u32[]{:S(2)}, u32[]{:S(2)}) collective-permute-start(bf16[512,384]{1,0:T(8,128)(2,1)S(1)} %constant_dynamic-update-slice_fusion), channel_id=1, source_target_pairs={{0,4},{1,5},{2,6},{3,7},{4,0},{5,1},{6,2},{7,3},{8,12},{9,13},{10,... | collective-permute-start | bytes 1179656 | tf_op jit(solution)/shard_map/ppermute | solution.py:42
  4.9 36.4 %collective-permute-start.5 = (bf16[512,384]{1,0:T(8,128)(2,1)S(1)}, bf16[512,384]{1,0:T(8,128)(2,1)S(1)}, u32[]{:S(2)}, u32[]{:S(2)}) collective-permute-start(bf16[512,384]{1,0:T(8,128)(2,1)S(1)} %constant_dynamic-update-slice_fusion), channel_id=1, source_target_pairs={{0,6},{1,7},{2,0},{3,1},{4,2},{5,3},{6,4},{7,5},{8,14},{9,15},{10,... | collective-permute-start | bytes 1179656 | tf_op jit(solution)/shard_map/ppermute | solution.py:42
  6.8 36.8 %collective-permute-start.8 = (bf16[96,4096]{1,0:T(8,128)(2,1)S(1)}, bf16[96,4096]{1,0:T(8,128)(2,1)S(1)}, u32[]{:S(2)}, u32[]{:S(2)}) collective-permute-start(bf16[96,4096]{1,0:T(8,128)(2,1)S(1)} %get-tuple-element.5), channel_id=1, source_target_pairs={{0,8},{8,0},{16,24},{24,16},{1,9},{9,1},{17,25},{25,17},{2,10},{10... | collective-permute-start | bytes 2359304 | tf_op jit(solution)/shard_map/ppermute | solution.py:42
  8.8 36.5 %copy-start = (bf16[1,192,4096]{2,1,0:T(8,128)(2,1)S(1)}, bf16[1,192,4096]{2,1,0:T(8,128)(2,1)}, u32[]{:S(2)}) copy-start(bf16[1,192,4096]{2,1,0:T(8,128)(2,1)} %param.5) | copy-start | bytes 4718596
  8.8 34.2 %collective-permute-start.9 = (bf16[96,4096]{1,0:T(8,128)(2,1)S(1)}, bf16[96,4096]{1,0:T(8,128)(2,1)S(1)}, u32[]{:S(2)}, u32[]{:S(2)}) collective-permute-start(bf16[96,4096]{1,0:T(8,128)(2,1)S(1)} %get-tuple-element.6), channel_id=1, source_target_pairs={{0,16},{8,24},{16,0},{24,8},{1,17},{9,25},{17,1},{25,9},{2,18},{10... | collective-permute-start | bytes 2359304 | tf_op jit(solution)/shard_map/ppermute | solution.py:42
  14.7 26.4 %collective-permute-start.2 = (bf16[512,384]{1,0:T(8,128)(2,1)}, bf16[512,384]{1,0:T(8,128)(2,1)S(1)}, u32[]{:S(2)}, u32[]{:S(2)}) collective-permute-start(bf16[512,384]{1,0:T(8,128)(2,1)} %collective-permute-done.1), channel_id=1, source_target_pairs={{0,1},{1,0},{2,3},{3,2},{4,5},{5,4},{6,7},{7,6},{8,9},{9,8},{10,11... | collective-permute-start | bytes 1179656 | tf_op jit(solution)/shard_map/ppermute | solution.py:42
  39.6 20.4 %collective-permute-start.7 = (bf16[96,4096]{1,0:T(8,128)(2,1)S(1)}, bf16[96,4096]{1,0:T(8,128)(2,1)S(1)}, u32[]{:S(2)}, u32[]{:S(2)}) collective-permute-start(bf16[96,4096]{1,0:T(8,128)(2,1)S(1)} %get-tuple-element.6), channel_id=1, source_target_pairs={{0,8},{8,0},{16,24},{24,16},{1,9},{9,1},{17,25},{25,17},{2,10},{10... | collective-permute-start | bytes 2359304 | tf_op jit(solution)/shard_map/ppermute | solution.py:42
  41.1 1.7 %collective-permute-start.4 = (bf16[512,384]{1,0:T(8,128)(2,1)S(1)}, bf16[512,384]{1,0:T(8,128)(2,1)S(1)}, u32[]{:S(2)}, u32[]{:S(2)}) collective-permute-start(bf16[512,384]{1,0:T(8,128)(2,1)S(1)} %collective-permute-done.3), channel_id=1, source_target_pairs={{0,1},{1,0},{2,3},{3,2},{4,5},{5,4},{6,7},{7,6},{8,9},{9,8},{10,11... | collective-permute-start | bytes 1179656 | tf_op jit(solution)/shard_map/ppermute | solution.py:42
  41.2 20.8 %collective-permute-start.10 = (bf16[96,4096]{1,0:T(8,128)(2,1)S(1)}, bf16[96,4096]{1,0:T(8,128)(2,1)S(1)}, u32[]{:S(2)}, u32[]{:S(2)}) collective-permute-start(bf16[96,4096]{1,0:T(8,128)(2,1)S(1)} %get-tuple-element.5), channel_id=1, source_target_pairs={{0,16},{8,24},{16,0},{24,8},{1,17},{9,25},{17,1},{25,9},{2,18},{10... | collective-permute-start | bytes 2359304 | tf_op jit(solution)/shard_map/ppermute | solution.py:42
  42.8 2.3 %collective-permute-start.6 = (bf16[512,384]{1,0:T(8,128)(2,1)S(1)}, bf16[512,384]{1,0:T(8,128)(2,1)S(1)}, u32[]{:S(2)}, u32[]{:S(2)}) collective-permute-start(bf16[512,384]{1,0:T(8,128)(2,1)S(1)} %collective-permute-done.5), channel_id=1, source_target_pairs={{0,1},{1,0},{2,3},{3,2},{4,5},{5,4},{6,7},{7,6},{8,9},{9,8},{10,11... | collective-permute-start | bytes 1179656 | tf_op jit(solution)/shard_map/ppermute | solution.py:42
  43.1 32.4 %collective-permute-start.11 = (bf16[96,4096]{1,0:T(8,128)(2,1)S(1)}, bf16[96,4096]{1,0:T(8,128)(2,1)S(1)}, u32[]{:S(2)}, u32[]{:S(2)}) collective-permute-start(bf16[96,4096]{1,0:T(8,128)(2,1)S(1)} %collective-permute-done.9), channel_id=1, source_target_pairs={{0,8},{8,0},{16,24},{24,16},{1,9},{9,1},{17,25},{25,17},{2,10},{10... | collective-permute-start | bytes 2359304 | tf_op jit(solution)/shard_map/ppermute | solution.py:42
  43.6 34.5 %collective-permute-start.12 = (bf16[96,4096]{1,0:T(8,128)(2,1)S(1)}, bf16[96,4096]{1,0:T(8,128)(2,1)S(1)}, u32[]{:S(2)}, u32[]{:S(2)}) collective-permute-start(bf16[96,4096]{1,0:T(8,128)(2,1)S(1)} %collective-permute-done.8), channel_id=1, source_target_pairs={{0,16},{8,24},{16,0},{24,8},{1,17},{9,25},{17,1},{25,9},{2,18},{10... | collective-permute-start | bytes 2359304 | tf_op jit(solution)/shard_map/ppermute | solution.py:42
  62.8 16.0 %slice-start = ((f32[1,1,768]{2,1,0:T(1,128)}), f32[1,1,512]{2,1,0:T(1,128)S(1)}, s32[]{:S(2)}) async-start(f32[1,1,768]{2,1,0:T(1,128)} %param.9), calls=%async_computation.1 | async-start | bytes 4096 | tf_op jit(solution)/shard_map/slice | solution.py:22
  78.8 0.9 %slice-start.1 = ((f32[1,1,768]{2,1,0:T(1,128)}), f32[1,1,256]{2,1,0:T(1,128)S(1)}, s32[]{:S(2)}) async-start(f32[1,1,768]{2,1,0:T(1,128)} %param.9), calls=%async_computation.2 | async-start | bytes 2048 | tf_op jit(solution)/shard_map/slice | solution.py:22

commit v2 on v1

v2 whole, which is shorter than its diff:
```python
import math

import jax
import jax.numpy as jnp
from jax import lax
from jax.sharding import PartitionSpec as P


block_rows = 1024


def attend(queries, keys, values, gates, places):
    length = queries.shape[0]
    scale = queries.shape[1] ** (-0.5)
    pieces = []
    for start in range(0, length, block_rows):
        finish = min(start + block_rows, length)
        scores = (
            jnp.dot(queries[start:finish], keys.T, preferred_element_type=jnp.float32) * scale
        )
        scores = scores + gates[start:finish, None] - gates[None, :]
        scores = jnp.where(places[None, :] <= places[start:finish, None], scores, -1e30)
        top = jnp.max(scores, axis=1, keepdims=True)
        weights = jnp.exp(scores - top)
        total = jnp.sum(weights, axis=1, keepdims=True)
        summed = jnp.dot(
            weights.astype(jnp.bfloat16), values, preferred_element_type=jnp.float32
        )
        pieces.append((summed / total).astype(jnp.bfloat16))
    return jnp.concatenate(pieces, axis=0)


def make_body(sp, dp):
    cores = 2
    planes = dp // cores
    side = math.isqrt(sp)

    def send(array, axis, count, target):
        return lax.ppermute(array, axis, [(i, target(i)) for i in range(count)])

    def shift(j, k):
        return lambda i: (i // side + j) % side * side + (i % side + k) % side

    def shift_z(k):
        return lambda i: (i + k * cores) % dp

    def twin_of(i):
        return i // cores * cores + (i + 1) % cores

    def body(tokens, query_weight, key_weight, value_weight, cum_gate):
        width = query_weight.shape[1]
        own = tokens[0]
        rows = own.shape[0]
        half, quarter = rows // 2, rows // 4
        s = lax.axis_index("sp")
        d = lax.axis_index("dp")
        y, x = s // side, s % side
        z, core = d // cores, d % cores
        local = jnp.concatenate([query_weight, key_weight, value_weight], axis=1)
        lower = [own[:quarter], own[quarter:half]]
        upper = [own[half : half + quarter], own[half + quarter :]]

        chunks = {(0, 0): [own]}
        early_y, early_x = {}, {}
        for k in range(1, side):
            early_x[k] = [send(part, "sp", sp, shift(0, k)) for part in upper]
            early_y[k] = [send(part, "sp", sp, shift(k, 0)) for part in lower]
            late_x = send(own[:half], "sp", sp, shift(0, k))
            late_y = send(own[half:], "sp", sp, shift(k, 0))
            chunks[(0, k)] = [late_x] + early_x[k]
            chunks[(k, 0)] = early_y[k] + [late_y]
        stripes = [local]
        for k in range(1, planes):
            stripes.append(send(local, "dp", dp, shift_z(k)))
        for j in range(1, side):
            for k in range(1, side):
                chunks[(j, k)] = [send(part, "sp", sp, shift(0, k)) for part in early_y[j]] + [
                    send(part, "sp", sp, shift(j, 0)) for part in early_x[k]
                ]
        whole = jnp.zeros((planes, cores) + local.shape, local.dtype)
        for k in range(planes):
            stripe = stripes[k]
            twin = send(stripe, "dp", dp, twin_of)
            at = (z - k) % planes
            whole = lax.dynamic_update_slice(whole, stripe[None, None], (at, core, 0, 0))
            whole = lax.dynamic_update_slice(whole, twin[None, None], (at, (core + 1) % cores, 0, 0))
        stacked = whole.reshape(dp * local.shape[0], local.shape[1])

        projected, gates, places = [], [], []
        for (j, k), parts in chunks.items():
            for part in parts:
                piece = jnp.dot(part, stacked, preferred_element_type=jnp.float32)
                projected.append(piece.astype(jnp.bfloat16))
            start = ((y - j) % side * side + (x - k) % side) * rows
            gates.append(lax.dynamic_slice(cum_gate[0, 0], (start,), (rows,)))
            places.append(start + lax.iota(jnp.int32, rows))
        projected = jnp.concatenate(projected, axis=0)
        queries = projected[:, :width]
        keys = projected[:, width : 2 * width]
        values = projected[:, 2 * width :]
        head_out = attend(queries, keys, values, jnp.concatenate(gates), jnp.concatenate(places))
        gathered = jnp.zeros((rows, sp * width), head_out.dtype)
        order = list(enumerate(chunks))
        for n, (j, k) in sorted(order, key=lambda entry: -sum(entry[1])):
            part = head_out[n * rows : (n + 1) * rows]
            if (j, k) != (0, 0):
                part = send(part, "sp", sp, shift(-j, -k))
            head = (y + j) % side * side + (x + k) % side
            gathered = lax.dynamic_update_slice(gathered, part, (0, head * width))
        return gathered[None]

    return body


def solution(mesh):
    in_specs = (
        P("dp", "sp", None),
        P("dp", "sp"),
        P("dp", "sp"),
        P("dp", "sp"),
        P("dp", "sp", None),
    )
    out_specs = P("dp", "sp", None)
    body = make_body(mesh.shape["sp"], mesh.shape["dp"])

    return jax.shard_map(body, mesh=mesh, in_specs=in_specs, out_specs=out_specs, check_vma=False)
```

time: 90.2 us -> 107 us (1.19)
  waiting for transfers between devices: 55 us -> 65.5 us
  blocking collectives: 8.14 us -> 0 us
  starting transfers between devices: 10.9 us -> 16.7 us
  local copies, waits for them, and re-layouts: 8.08 us -> 12.5 us
  matrix products: 7.02 us -> 9.29 us
  other arithmetic: 0.51 us -> 2.59 us
    ppermute x13 -> x20, waiting for transfers between devices: 55 us -> 65.5 us  [send(): return lax.ppermute(array, axis, [(i, target(i)) for i in range(count)])]
    all_to_all x1 -> x0, blocking collectives: 8.14 us -> none  [body(): lax.all_to_all(head_out, 'sp', split_axis=0, concat_axis=1, tiled=True)]
    ppermute x13 -> x20, starting transfers between devices: 10.9 us -> 16.7 us  [send(): return lax.ppermute(array, axis, [(i, target(i)) for i in range(count)])]
    dot_general x8 -> x11, matrix products: 5.51 us -> 8.08 us  [body(): piece = jnp.dot(part, stacked, preferred_element_type=jnp.float32)]
    dynamic_update_slice x4, local copies, waits for them, and re-layouts: 1.27 us -> 3.26 us  [body(): lax.dynamic_update_slice(whole, stripe[None, None], (at, core, 0, 0))]
    concatenate x1 -> x2, other arithmetic: 0.02 us -> 1.62 us  [the longest x1 0.85 us: body(): jnp.concatenate(gates)]
    slice x5 -> x3, local copies, waits for them, and re-layouts: 1.49 us -> 2.71 us  [the longest x1 1.51 us: body(): late_y = send(own[half:], 'sp', sp, shift(k, 0))]
    unnamed x6 -> x16, local copies, waits for them, and re-layouts: 1.89 us -> 2.68 us
  transfers between devices with their start and end apart: 13 -> 20, of which waited for: 5 -> 11; matrix products, arithmetic and copies ran while one was open for 10% -> 17% of each run, Pallas kernels for 0% -> 0%
where the time goes in v2:
time: 107 us
  waiting for transfers between devices  65.5 us (61%)
  starting transfers between devices  16.7 us (16%)
  local copies, waits for them, and re-layouts  12.5 us (12%)
  matrix products  9.29 us (9%)
  other arithmetic  2.59 us (2%)
    ppermute x20, waiting for transfers between devices, send(): return lax.ppermute(array, axis, [(i, target(i)) for i in range(count)])  65.5 us
    ppermute x20, starting transfers between devices, send(): return lax.ppermute(array, axis, [(i, target(i)) for i in range(count)])  16.7 us
    dot_general x11, matrix products, body(): piece = jnp.dot(part, stacked, preferred_element_type=jnp.float32)  8.08 us
    dynamic_update_slice x4, local copies, waits for them, and re-layouts, body(): lax.dynamic_update_slice(whole, stripe[None, None], (at, core, 0, 0))  3.26 us
    unnamed x16, local copies, waits for them, and re-layouts  2.68 us
  transfers between devices with their start and end apart: 20, of which 11 were waited for; matrix products, arithmetic and copies ran while one was open for 17% of the time, Pallas kernels for 0%

profile of v2, /device:TPU:24, one launch (start us, length us, event | category | flops | bytes accessed | tf_op | source)
XLA Modules:
  0.0 106.8 jit_solution(14982008307315027659)
XLA Ops:
  0.0 1.0 constant_dynamic-update-slice_fusion.2
  1.1 0.9 constant_dynamic-update-slice_fusion.1
  2.0 0.9 constant_dynamic-update-slice_fusion
  3.1 1.9 %collective-permute-start.3 = (bf16[512,384]{1,0:T(8,128)(2,1)S(1)}, bf16[512,384]{1,0:T(8,128)(2,1)}, u32[]{:S(2)}, u32[]{:S(2)}) collective-permute-start(bf16[512,384]{1,0:T(8,128)(2,1)S(1)} %constant_dynamic-update-slice_fusion), channel_id=1, source_target_pairs={{0,4},{1,5},{2,6},{3,7},{4,0},{5,1},{6,2},{7,3},{8,12},{9,13},{10,... | collective-permute-start | bytes 1179656 | tf_op jit(solution)/shard_map/ppermute | solution.py:39
  5.4 1.5 %slice_bitcast_fusion = (bf16[96,4096]{1,0:T(8,128)(2,1)S(1)}, bf16[96,4096]{1,0:T(8,128)(2,1)S(1)}) fusion(bf16[1,192,4096]{2,1,0:T(8,128)(2,1)} %param.5), kind=kLoop, calls=%fused_computation.42 | loop fusion | bytes 3145728 | tf_op jit(solution)/shard_map/slice | solution.py:69
  7.0 1.6 %collective-permute-start.7 = (bf16[96,4096]{1,0:T(8,128)(2,1)S(1)}, bf16[96,4096]{1,0:T(8,128)(2,1)}, u32[]{:S(2)}, u32[]{:S(2)}) collective-permute-start(bf16[96,4096]{1,0:T(8,128)(2,1)S(1)} %get-tuple-element.6), channel_id=1, source_target_pairs={{0,8},{8,0},{16,24},{24,16},{1,9},{9,1},{17,25},{25,17},{2,10},{10... | collective-permute-start | bytes 2359304 | tf_op jit(solution)/shard_map/ppermute | solution.py:39
  8.5 1.2 %slice_bitcast_fusion.2 = (bf16[48,4096]{1,0:T(8,128)(2,1)}, bf16[48,4096]{1,0:T(8,128)(2,1)}, bf16[48,4096]{1,0:T(8,128)(2,1)}, bf16[48,4096]{1,0:T(8,128)(2,1)}) fusion(bf16[1,192,4096]{2,1,0:T(8,128)(2,1)S(1)} %copy-done), kind=kLoop, calls=%fused_computation.52 | loop fusion | bytes 3145728 | tf_op jit(solution)/shard_map/slice | solution.py:60
  9.7 0.6 iota_add_fusion.2
  10.3 0.8 pad_add_fusion
  11.1 0.7 constant_dynamic-slice_fusion.3
  11.8 0.8 pad_maximum_fusion
  13.0 0.6 collective-permute-start.8
  13.6 1.2 %collective-permute-done.1 = bf16[512,384]{1,0:T(8,128)(2,1)} collective-permute-done((bf16[512,384]{1,0:T(8,128)(2,1)S(1)}, bf16[512,384]{1,0:T(8,128)(2,1)}, u32[]{:S(2)}, u32[]{:S(2)}) %collective-permute-start.1) | collective-permute-done | bytes 393248 | tf_op jit(solution)/shard_map/ppermute | solution.py:39
  14.8 1.1 bitcast_dynamic-update-slice_fusion.6
  15.9 1.1 bitcast_dynamic-update-slice_fusion.5
  17.0 22.9 %collective-permute-done.3 = bf16[512,384]{1,0:T(8,128)(2,1)} collective-permute-done((bf16[512,384]{1,0:T(8,128)(2,1)S(1)}, bf16[512,384]{1,0:T(8,128)(2,1)}, u32[]{:S(2)}, u32[]{:S(2)}) %collective-permute-start.3) | collective-permute-done | bytes 393248 | tf_op jit(solution)/shard_map/ppermute | solution.py:39
  39.8 1.5 %collective-permute-start.9 = (bf16[48,4096]{1,0:T(8,128)(2,1)S(1)}, bf16[48,4096]{1,0:T(8,128)(2,1)S(1)}, u32[]{:S(2)}, u32[]{:S(2)}) collective-permute-start(bf16[48,4096]{1,0:T(8,128)(2,1)S(1)} %copy-done.1), channel_id=1, source_target_pairs={{0,8},{8,0},{16,24},{24,16},{1,9},{9,1},{17,25},{25,17},{2,10},{10... | collective-permute-start | bytes 1179656 | tf_op jit(solution)/shard_map/ppermute | solution.py:39
  41.4 1.1 bitcast_dynamic-update-slice_fusion.3
  42.5 1.6 %collective-permute-start.10 = (bf16[48,4096]{1,0:T(8,128)(2,1)S(1)}, bf16[48,4096]{1,0:T(8,128)(2,1)S(1)}, u32[]{:S(2)}, u32[]{:S(2)}) collective-permute-start(bf16[48,4096]{1,0:T(8,128)(2,1)S(1)} %copy-done.3), channel_id=1, source_target_pairs={{0,16},{8,24},{16,0},{24,8},{1,17},{9,25},{17,1},{25,9},{2,18},{10... | collective-permute-start | bytes 1179656 | tf_op jit(solution)/shard_map/ppermute | solution.py:39
  44.4 1.1 bitcast_dynamic-update-slice_fusion.1
  45.4 0.6 collective-permute-done.6
  46.0 0.7 collective-permute-start.11
  46.8 1.0 fusion.15
  47.8 1.4 %collective-permute-start.12 = (bf16[96,4096]{1,0:T(8,128)(2,1)S(1)}, bf16[96,4096]{1,0:T(8,128)(2,1)S(1)}, u32[]{:S(2)}, u32[]{:S(2)}) collective-permute-start(bf16[96,4096]{1,0:T(8,128)(2,1)S(1)} %get-tuple-element.5), channel_id=1, source_target_pairs={{0,16},{8,24},{16,0},{24,8},{1,17},{9,25},{17,1},{25,9},{2,18},{10... | collective-permute-start | bytes 2359304 | tf_op jit(solution)/shard_map/ppermute | solution.py:39
  49.2 5.3 %collective-permute-done.10 = bf16[48,4096]{1,0:T(8,128)(2,1)S(1)} collective-permute-done((bf16[48,4096]{1,0:T(8,128)(2,1)S(1)}, bf16[48,4096]{1,0:T(8,128)(2,1)S(1)}, u32[]{:S(2)}, u32[]{:S(2)}) %collective-permute-start.10) | collective-permute-done | bytes 393248 | tf_op jit(solution)/shard_map/ppermute | solution.py:39
  55.1 7.9 %collective-permute-done.11 = bf16[48,4096]{1,0:T(8,128)(2,1)S(1)} collective-permute-done((bf16[48,4096]{1,0:T(8,128)(2,1)S(1)}, bf16[48,4096]{1,0:T(8,128)(2,1)S(1)}, u32[]{:S(2)}, u32[]{:S(2)}) %collective-permute-start.11) | collective-permute-done | bytes 393248 | tf_op jit(solution)/shard_map/ppermute | solution.py:39
  63.5 1.5 %collective-permute-start.15 = (bf16[48,4096]{1,0:T(8,128)(2,1)S(1)}, bf16[48,4096]{1,0:T(8,128)(2,1)S(1)}, u32[]{:S(2)}, u32[]{:S(2)}) collective-permute-start(bf16[48,4096]{1,0:T(8,128)(2,1)S(1)} %collective-permute-done.8), channel_id=1, source_target_pairs={{0,16},{8,24},{16,0},{24,8},{1,17},{9,25},{17,1},{25,9},{2,18},{10... | collective-permute-start | bytes 1179656 | tf_op jit(solution)/shard_map/ppermute | solution.py:39
  65.5 1.8 %fusion.19 = bf16[768,384]{1,0:T(8,128)(2,1)S(1)} fusion(bf16[768,384]{1,0:T(8,128)(2,1)S(1)} %fusion.15, bf16[96,4096]{1,0:T(8,128)(2,1)} %collective-permute-done.7, bf16[4096,384]{1,0:T(8,128)(2,1)S(1)} %bitcast.118), kind=kOutput, calls=%fused_computation.15 | convolution fusion | flops 302026752 | bytes 4005888 | tf_op jit(solution)/shard_map/dot_general | solution.py:92
  67.3 0.6 fusion.23
  67.9 0.6 fusion.25
  68.5 0.6 fusion.27
  69.1 0.6 fusion.29
  69.6 10.2 %collective-permute-done.12 = bf16[96,4096]{1,0:T(8,128)(2,1)S(1)} collective-permute-done((bf16[96,4096]{1,0:T(8,128)(2,1)S(1)}, bf16[96,4096]{1,0:T(8,128)(2,1)S(1)}, u32[]{:S(2)}, u32[]{:S(2)}) %collective-permute-start.12) | collective-permute-done | bytes 786464 | tf_op jit(solution)/shard_map/ppermute | solution.py:39
  79.8 0.7 fusion.21
  80.5 0.6 fusion.31
  81.1 0.6 fusion.33
  81.7 6.6 %collective-permute-done.15 = bf16[48,4096]{1,0:T(8,128)(2,1)S(1)} collective-permute-done((bf16[48,4096]{1,0:T(8,128)(2,1)S(1)}, bf16[48,4096]{1,0:T(8,128)(2,1)S(1)}, u32[]{:S(2)}, u32[]{:S(2)}) %collective-permute-start.15) | collective-permute-done | bytes 393248 | tf_op jit(solution)/shard_map/ppermute | solution.py:39
  88.2 0.6 fusion.35
  88.8 7.4 %collective-permute-done.16 = bf16[48,4096]{1,0:T(8,128)(2,1)S(1)} collective-permute-done((bf16[48,4096]{1,0:T(8,128)(2,1)S(1)}, bf16[48,4096]{1,0:T(8,128)(2,1)S(1)}, u32[]{:S(2)}, u32[]{:S(2)}) %collective-permute-start.16) | collective-permute-done | bytes 393248 | tf_op jit(solution)/shard_map/ppermute | solution.py:39
  96.2 0.6 fusion.37
  96.8 0.7 fusion.43
  97.8 0.5 fusion.6
  98.4 1.6 %collective-permute-start.17 = (bf16[192,128]{1,0:T(8,128)(2,1)S(1)}, bf16[192,128]{1,0:T(8,128)(2,1)S(1)}, u32[]{:S(2)}, u32[]{:S(2)}) collective-permute-start(bf16[192,128]{1,0:T(8,128)(2,1)S(1)} %get-tuple-element.13), channel_id=1, source_target_pairs={{0,24},{8,16},{16,8},{24,0},{1,25},{9,17},{17,9},{25,1},{2,26},{10... | collective-permute-start | bytes 147464 | tf_op jit(solution)/shard_map/ppermute | solution.py:39
  99.9 1.5 %collective-permute-start.18 = (bf16[192,128]{1,0:T(8,128)(2,1)S(1)}, bf16[192,128]{1,0:T(8,128)(2,1)S(1)}, u32[]{:S(2)}, u32[]{:S(2)}) collective-permute-start(bf16[192,128]{1,0:T(8,128)(2,1)S(1)} %get-tuple-element.12), channel_id=1, source_target_pairs={{0,8},{8,0},{16,24},{24,16},{1,9},{9,1},{17,25},{25,17},{2,10},{10... | collective-permute-start | bytes 147464 | tf_op jit(solution)/shard_map/ppermute | solution.py:39
  101.9 1.5 %collective-permute-done.17 = bf16[192,128]{1,0:T(8,128)(2,1)S(1)} collective-permute-done((bf16[192,128]{1,0:T(8,128)(2,1)S(1)}, bf16[192,128]{1,0:T(8,128)(2,1)S(1)}, u32[]{:S(2)}, u32[]{:S(2)}) %collective-permute-start.17) | collective-permute-done | bytes 49184 | tf_op jit(solution)/shard_map/ppermute | solution.py:39
  104.0 1.5 %collective-permute-done.19 = bf16[192,128]{1,0:T(8,128)(2,1)S(1)} collective-permute-done((bf16[192,128]{1,0:T(8,128)(2,1)S(1)}, bf16[192,128]{1,0:T(8,128)(2,1)S(1)}, u32[]{:S(2)}, u32[]{:S(2)}) %collective-permute-start.19) | collective-permute-done | bytes 49184 | tf_op jit(solution)/shard_map/ppermute | solution.py:39
  105.6 0.7 copy-done.5
  106.2 0.6 fusion.41
  (45 shorter events, 4.4 us)
Async XLA Ops:
  0.0 8.5 %copy-start = (bf16[1,192,4096]{2,1,0:T(8,128)(2,1)S(1)}, bf16[1,192,4096]{2,1,0:T(8,128)(2,1)}, u32[]{:S(2)}) copy-start(bf16[1,192,4096]{2,1,0:T(8,128)(2,1)} %param.5) | copy-start | bytes 4718596
  2.9 8.2 %copy-start.6 = (f32[1,1,768]{2,1,0:T(1,128)S(1)}, f32[1,1,768]{2,1,0:T(1,128)}, u32[]{:S(2)}) copy-start(f32[1,1,768]{2,1,0:T(1,128)} %param.9) | copy-start | bytes 9220
  2.9 10.0 %collective-permute-start = (bf16[512,384]{1,0:T(8,128)(2,1)S(1)}, bf16[512,384]{1,0:T(8,128)(2,1)}, u32[]{:S(2)}, u32[]{:S(2)}) collective-permute-start(bf16[512,384]{1,0:T(8,128)(2,1)S(1)} %constant_dynamic-update-slice_fusion), channel_id=1, source_target_pairs={{0,1},{1,0},{2,3},{3,2},{4,5},{5,4},{6,7},{7,6},{8,9},{9,8},{10,11... | collective-permute-start | bytes 1179656 | tf_op jit(solution)/shard_map/ppermute | solution.py:39
  3.0 11.8 %collective-permute-start.1 = (bf16[512,384]{1,0:T(8,128)(2,1)S(1)}, bf16[512,384]{1,0:T(8,128)(2,1)}, u32[]{:S(2)}, u32[]{:S(2)}) collective-permute-start(bf16[512,384]{1,0:T(8,128)(2,1)S(1)} %constant_dynamic-update-slice_fusion), channel_id=1, source_target_pairs={{0,2},{1,3},{2,4},{3,5},{4,6},{5,7},{6,0},{7,1},{8,10},{9,11},{10,... | collective-permute-start | bytes 1179656 | tf_op jit(solution)/shard_map/ppermute | solution.py:39
  3.1 36.7 %collective-permute-start.3 = (bf16[512,384]{1,0:T(8,128)(2,1)S(1)}, bf16[512,384]{1,0:T(8,128)(2,1)}, u32[]{:S(2)}, u32[]{:S(2)}) collective-permute-start(bf16[512,384]{1,0:T(8,128)(2,1)S(1)} %constant_dynamic-update-slice_fusion), channel_id=1, source_target_pairs={{0,4},{1,5},{2,6},{3,7},{4,0},{5,1},{6,2},{7,3},{8,12},{9,13},{10,... | collective-permute-start | bytes 1179656 | tf_op jit(solution)/shard_map/ppermute | solution.py:39
  5.0 37.5 %collective-permute-start.5 = (bf16[512,384]{1,0:T(8,128)(2,1)S(1)}, bf16[512,384]{1,0:T(8,128)(2,1)}, u32[]{:S(2)}, u32[]{:S(2)}) collective-permute-start(bf16[512,384]{1,0:T(8,128)(2,1)S(1)} %constant_dynamic-update-slice_fusion), channel_id=1, source_target_pairs={{0,6},{1,7},{2,0},{3,1},{4,2},{5,3},{6,4},{7,5},{8,14},{9,15},{10,... | collective-permute-start | bytes 1179656 | tf_op jit(solution)/shard_map/ppermute | solution.py:39
  7.0 58.1 %collective-permute-start.7 = (bf16[96,4096]{1,0:T(8,128)(2,1)S(1)}, bf16[96,4096]{1,0:T(8,128)(2,1)}, u32[]{:S(2)}, u32[]{:S(2)}) collective-permute-start(bf16[96,4096]{1,0:T(8,128)(2,1)S(1)} %get-tuple-element.6), channel_id=1, source_target_pairs={{0,8},{8,0},{16,24},{24,16},{1,9},{9,1},{17,25},{25,17},{2,10},{10... | collective-permute-start | bytes 2359304 | tf_op jit(solution)/shard_map/ppermute | solution.py:39
  11.8 1.2 %copy-start.4 = (bf16[48,4096]{1,0:T(8,128)(2,1)S(1)}, bf16[48,4096]{1,0:T(8,128)(2,1)}, u32[]{:S(2)}) copy-start(bf16[48,4096]{1,0:T(8,128)(2,1)} %get-tuple-element.10) | copy-start | bytes 1179652
  11.8 28.0 %copy-start.1 = (bf16[48,4096]{1,0:T(8,128)(2,1)S(1)}, bf16[48,4096]{1,0:T(8,128)(2,1)}, u32[]{:S(2)}) copy-start(bf16[48,4096]{1,0:T(8,128)(2,1)} %get-tuple-element.9) | copy-start | bytes 1179652
  12.6 29.8 %copy-start.3 = (bf16[48,4096]{1,0:T(8,128)(2,1)S(1)}, bf16[48,4096]{1,0:T(8,128)(2,1)}, u32[]{:S(2)}) copy-start(bf16[48,4096]{1,0:T(8,128)(2,1)} %get-tuple-element.8) | copy-start | bytes 1179652
  12.9 33.1 %copy-start.2 = (bf16[48,4096]{1,0:T(8,128)(2,1)S(1)}, bf16[48,4096]{1,0:T(8,128)(2,1)}, u32[]{:S(2)}) copy-start(bf16[48,4096]{1,0:T(8,128)(2,1)} %get-tuple-element.7) | copy-start | bytes 1179652
  13.0 34.8 %collective-permute-start.8 = (bf16[48,4096]{1,0:T(8,128)(2,1)S(1)}, bf16[48,4096]{1,0:T(8,128)(2,1)S(1)}, u32[]{:S(2)}, u32[]{:S(2)}) collective-permute-start(bf16[48,4096]{1,0:T(8,128)(2,1)S(1)} %copy-done.4), channel_id=1, source_target_pairs={{0,8},{8,0},{16,24},{24,16},{1,9},{9,1},{17,25},{25,17},{2,10},{10... | collective-permute-start | bytes 1179656 | tf_op jit(solution)/shard_map/ppermute | solution.py:39
  14.8 26.5 %collective-permute-start.2 = (bf16[512,384]{1,0:T(8,128)(2,1)}, bf16[512,384]{1,0:T(8,128)(2,1)S(1)}, u32[]{:S(2)}, u32[]{:S(2)}) collective-permute-start(bf16[512,384]{1,0:T(8,128)(2,1)} %collective-permute-done.1), channel_id=1, source_target_pairs={{0,1},{1,0},{2,3},{3,2},{4,5},{5,4},{6,7},{7,6},{8,9},{9,8},{10,11... | collective-permute-start | bytes 1179656 | tf_op jit(solution)/shard_map/ppermute | solution.py:39
  39.8 23.7 %collective-permute-start.9 = (bf16[48,4096]{1,0:T(8,128)(2,1)S(1)}, bf16[48,4096]{1,0:T(8,128)(2,1)S(1)}, u32[]{:S(2)}, u32[]{:S(2)}) collective-permute-start(bf16[48,4096]{1,0:T(8,128)(2,1)S(1)} %copy-done.1), channel_id=1, source_target_pairs={{0,8},{8,0},{16,24},{24,16},{1,9},{9,1},{17,25},{25,17},{2,10},{10... | collective-permute-start | bytes 1179656 | tf_op jit(solution)/shard_map/ppermute | solution.py:39
  41.3 2.7 %collective-permute-start.4 = (bf16[512,384]{1,0:T(8,128)(2,1)}, bf16[512,384]{1,0:T(8,128)(2,1)S(1)}, u32[]{:S(2)}, u32[]{:S(2)}) collective-permute-start(bf16[512,384]{1,0:T(8,128)(2,1)} %collective-permute-done.3), channel_id=1, source_target_pairs={{0,1},{1,0},{2,3},{3,2},{4,5},{5,4},{6,7},{7,6},{8,9},{9,8},{10,11... | collective-permute-start | bytes 1179656 | tf_op jit(solution)/shard_map/ppermute | solution.py:39
  42.5 12.1 %collective-permute-start.10 = (bf16[48,4096]{1,0:T(8,128)(2,1)S(1)}, bf16[48,4096]{1,0:T(8,128)(2,1)S(1)}, u32[]{:S(2)}, u32[]{:S(2)}) collective-permute-start(bf16[48,4096]{1,0:T(8,128)(2,1)S(1)} %copy-done.3), channel_id=1, source_target_pairs={{0,16},{8,24},{16,0},{24,8},{1,17},{9,25},{17,1},{25,9},{2,18},{10... | collective-permute-start | bytes 1179656 | tf_op jit(solution)/shard_map/ppermute | solution.py:39
  44.1 1.9 %collective-permute-start.6 = (bf16[512,384]{1,0:T(8,128)(2,1)}, bf16[512,384]{1,0:T(8,128)(2,1)S(1)}, u32[]{:S(2)}, u32[]{:S(2)}) collective-permute-start(bf16[512,384]{1,0:T(8,128)(2,1)} %collective-permute-done.5), channel_id=1, source_target_pairs={{0,1},{1,0},{2,3},{3,2},{4,5},{5,4},{6,7},{7,6},{8,9},{9,8},{10,11... | collective-permute-start | bytes 1179656 | tf_op jit(solution)/shard_map/ppermute | solution.py:39
  46.0 17.0 %collective-permute-start.11 = (bf16[48,4096]{1,0:T(8,128)(2,1)S(1)}, bf16[48,4096]{1,0:T(8,128)(2,1)S(1)}, u32[]{:S(2)}, u32[]{:S(2)}) collective-permute-start(bf16[48,4096]{1,0:T(8,128)(2,1)S(1)} %copy-done.2), channel_id=1, source_target_pairs={{0,16},{8,24},{16,0},{24,8},{1,17},{9,25},{17,1},{25,9},{2,18},{10... | collective-permute-start | bytes 1179656 | tf_op jit(solution)/shard_map/ppermute | solution.py:39
  47.8 32.0 %collective-permute-start.12 = (bf16[96,4096]{1,0:T(8,128)(2,1)S(1)}, bf16[96,4096]{1,0:T(8,128)(2,1)S(1)}, u32[]{:S(2)}, u32[]{:S(2)}) collective-permute-start(bf16[96,4096]{1,0:T(8,128)(2,1)S(1)} %get-tuple-element.5), channel_id=1, source_target_pairs={{0,16},{8,24},{16,0},{24,8},{1,17},{9,25},{17,1},{25,9},{2,18},{10... | collective-permute-start | bytes 2359304 | tf_op jit(solution)/shard_map/ppermute | solution.py:39
  54.5 26.0 %collective-permute-start.13 = (bf16[48,4096]{1,0:T(8,128)(2,1)S(1)}, bf16[48,4096]{1,0:T(8,128)(2,1)S(1)}, u32[]{:S(2)}, u32[]{:S(2)}) collective-permute-start(bf16[48,4096]{1,0:T(8,128)(2,1)S(1)} %collective-permute-done.10), channel_id=1, source_target_pairs={{0,8},{8,0},{16,24},{24,16},{1,9},{9,1},{17,25},{25,17},{2,10},{10... | collective-permute-start | bytes 1179656 | tf_op jit(solution)/shard_map/ppermute | solution.py:39
  63.0 18.1 %collective-permute-start.14 = (bf16[48,4096]{1,0:T(8,128)(2,1)S(1)}, bf16[48,4096]{1,0:T(8,128)(2,1)S(1)}, u32[]{:S(2)}, u32[]{:S(2)}) collective-permute-start(bf16[48,4096]{1,0:T(8,128)(2,1)S(1)} %collective-permute-done.11), channel_id=1, source_target_pairs={{0,8},{8,0},{16,24},{24,16},{1,9},{9,1},{17,25},{25,17},{2,10},{10... | collective-permute-start | bytes 1179656 | tf_op jit(solution)/shard_map/ppermute | solution.py:39
  63.5 24.7 %collective-permute-start.15 = (bf16[48,4096]{1,0:T(8,128)(2,1)S(1)}, bf16[48,4096]{1,0:T(8,128)(2,1)S(1)}, u32[]{:S(2)}, u32[]{:S(2)}) collective-permute-start(bf16[48,4096]{1,0:T(8,128)(2,1)S(1)} %collective-permute-done.8), channel_id=1, source_target_pairs={{0,16},{8,24},{16,0},{24,8},{1,17},{9,25},{17,1},{25,9},{2,18},{10... | collective-permute-start | bytes 1179656 | tf_op jit(solution)/shard_map/ppermute | solution.py:39
  65.0 31.2 %collective-permute-start.16 = (bf16[48,4096]{1,0:T(8,128)(2,1)S(1)}, bf16[48,4096]{1,0:T(8,128)(2,1)S(1)}, u32[]{:S(2)}, u32[]{:S(2)}) collective-permute-start(bf16[48,4096]{1,0:T(8,128)(2,1)S(1)} %collective-permute-done.9), channel_id=1, source_target_pairs={{0,16},{8,24},{16,0},{24,8},{1,17},{9,25},{17,1},{25,9},{2,18},{10... | collective-permute-start | bytes 1179656 | tf_op jit(solution)/shard_map/ppermute | solution.py:39
  98.4 5.1 %collective-permute-start.17 = (bf16[192,128]{1,0:T(8,128)(2,1)S(1)}, bf16[192,128]{1,0:T(8,128)(2,1)S(1)}, u32[]{:S(2)}, u32[]{:S(2)}) collective-permute-start(bf16[192,128]{1,0:T(8,128)(2,1)S(1)} %get-tuple-element.13), channel_id=1, source_target_pairs={{0,24},{8,16},{16,8},{24,0},{1,25},{9,17},{17,9},{25,1},{2,26},{10... | collective-permute-start | bytes 147464 | tf_op jit(solution)/shard_map/ppermute | solution.py:39
  99.9 4.1 %collective-permute-start.18 = (bf16[192,128]{1,0:T(8,128)(2,1)S(1)}, bf16[192,128]{1,0:T(8,128)(2,1)S(1)}, u32[]{:S(2)}, u32[]{:S(2)}) collective-permute-start(bf16[192,128]{1,0:T(8,128)(2,1)S(1)} %get-tuple-element.12), channel_id=1, source_target_pairs={{0,8},{8,0},{16,24},{24,16},{1,9},{9,1},{17,25},{25,17},{2,10},{10... | collective-permute-start | bytes 147464 | tf_op jit(solution)/shard_map/ppermute | solution.py:39
  101.4 4.1 %collective-permute-start.19 = (bf16[192,128]{1,0:T(8,128)(2,1)S(1)}, bf16[192,128]{1,0:T(8,128)(2,1)S(1)}, u32[]{:S(2)}, u32[]{:S(2)}) collective-permute-start(bf16[192,128]{1,0:T(8,128)(2,1)S(1)} %get-tuple-element.11), channel_id=1, source_target_pairs={{0,16},{8,24},{16,0},{24,8},{1,17},{9,25},{17,1},{25,9},{2,18},{10... | collective-permute-start | bytes 147464 | tf_op jit(solution)/shard_map/ppermute | solution.py:39
  105.5 0.7 copy-start.5

commit v3 on v2

--- a/solution.py
+++ b/solution.py
@@ -51,32 +51,28 @@
         width = query_weight.shape[1]
         own = tokens[0]
         rows = own.shape[0]
-        half, quarter = rows // 2, rows // 4
+        half = rows // 2
         s = lax.axis_index("sp")
         d = lax.axis_index("dp")
         y, x = s // side, s % side
         z, core = d // cores, d % cores
         local = jnp.concatenate([query_weight, key_weight, value_weight], axis=1)
-        lower = [own[:quarter], own[quarter:half]]
-        upper = [own[half : half + quarter], own[half + quarter :]]
 
-        chunks = {(0, 0): [own]}
-        early_y, early_x = {}, {}
+        chunks = {(0, 0): own}
+        lower = {}
         for k in range(1, side):
-            early_x[k] = [send(part, "sp", sp, shift(0, k)) for part in upper]
-            early_y[k] = [send(part, "sp", sp, shift(k, 0)) for part in lower]
-            late_x = send(own[:half], "sp", sp, shift(0, k))
-            late_y = send(own[half:], "sp", sp, shift(k, 0))
-            chunks[(0, k)] = [late_x] + early_x[k]
-            chunks[(k, 0)] = early_y[k] + [late_y]
+            chunks[(0, k)] = send(own, "sp", sp, shift(0, k))
+            lower[k] = send(own[:half], "sp", sp, shift(k, 0))
+            upper = send(own[half:], "sp", sp, shift(k, 0))
+            chunks[(k, 0)] = jnp.concatenate([lower[k], upper], axis=0)
         stripes = [local]
         for k in range(1, planes):
             stripes.append(send(local, "dp", dp, shift_z(k)))
         for j in range(1, side):
             for k in range(1, side):
-                chunks[(j, k)] = [send(part, "sp", sp, shift(0, k)) for part in early_y[j]] + [
-                    send(part, "sp", sp, shift(j, 0)) for part in early_x[k]
-                ]
+                first = send(lower[j], "sp", sp, shift(0, k))
+                second = send(chunks[(0, k)][half:], "sp", sp, shift(j, 0))
+                chunks[(j, k)] = jnp.concatenate([first, second], axis=0)
         whole = jnp.zeros((planes, cores) + local.shape, local.dtype)
         for k in range(planes):
             stripe = stripes[k]
@@ -87,10 +83,9 @@
         stacked = whole.reshape(dp * local.shape[0], local.shape[1])
 
         projected, gates, places = [], [], []
-        for (j, k), parts in chunks.items():
-            for part in parts:
-                piece = jnp.dot(part, stacked, preferred_element_type=jnp.float32)
-                projected.append(piece.astype(jnp.bfloat16))
+        for (j, k), part in chunks.items():
+            piece = jnp.dot(part, stacked, preferred_element_type=jnp.float32)
+            projected.append(piece.astype(jnp.bfloat16))
             start = ((y - j) % side * side + (x - k) % side) * rows
             gates.append(lax.dynamic_slice(cum_gate[0, 0], (start,), (rows,)))
             places.append(start + lax.iota(jnp.int32, rows))

time: 107 us -> 87.1 us (0.81)
  waiting for transfers between devices: 65.5 us -> 55.6 us
  starting transfers between devices: 16.7 us -> 13.3 us
  matrix products: 9.29 us -> 6.4 us
  other arithmetic: 2.59 us -> 0.59 us
  local copies, waits for them, and re-layouts: 12.5 us -> 10.6 us
    ppermute x20 -> x15, waiting for transfers between devices: 65.5 us -> 55.6 us  [send(): return lax.ppermute(array, axis, [(i, target(i)) for i in range(count)])]
    ppermute x20 -> x15, starting transfers between devices: 16.7 us -> 13.3 us  [send(): return lax.ppermute(array, axis, [(i, target(i)) for i in range(count)])]
    dot_general x11 -> x4, matrix products: 8.08 us -> 5.19 us  [body(): piece = jnp.dot(part, stacked, preferred_element_type=jnp.float32)]
    slice x2, local copies, waits for them, and re-layouts: 2.7 us -> 1.52 us  [the longest x1 1.47 us: body(): upper = send(own[half:], 'sp', sp, shift(k, 0))]
    unnamed x16 -> x8, local copies, waits for them, and re-layouts: 2.68 us -> 2.56 us
  transfers between devices with their start and end apart: 20 -> 15, of which waited for: 11 -> 7; matrix products, arithmetic and copies ran while one was open for 17% -> 12% of each run, Pallas kernels for 0% -> 0%
where the time goes in v3:
time: 87.1 us; the launch traced here: 86.7 us
  waiting for transfers between devices  55.6 us (64%)
  starting transfers between devices  13.3 us (15%)
  local copies, waits for them, and re-layouts  10.6 us (12%)
  matrix products  6.4 us (7%)
    ppermute x15, waiting for transfers between devices, send(): return lax.ppermute(array, axis, [(i, target(i)) for i in range(count)])  55.6 us
    ppermute x15, starting transfers between devices, send(): return lax.ppermute(array, axis, [(i, target(i)) for i in range(count)])  13.3 us
    dot_general x4, matrix products, body(): piece = jnp.dot(part, stacked, preferred_element_type=jnp.float32)  5.19 us
    dynamic_update_slice x4, local copies, waits for them, and re-layouts, body(): lax.dynamic_update_slice(whole, stripe[None, None], (at, core, 0, 0))  3.26 us
    unnamed x8, local copies, waits for them, and re-layouts  2.56 us
  transfers between devices with their start and end apart: 15, of which 7 were waited for; matrix products, arithmetic and copies ran while one was open for 12% of the time, Pallas kernels for 0%

profile of v3, /device:TPU:24, one launch (start us, length us, event | category | flops | bytes accessed | tf_op | source)
XLA Modules:
  0.0 86.7 jit_solution(18056641787043601649)
XLA Ops:
  0.0 0.9 %constant_dynamic-update-slice_fusion.2 = bf16[512,384]{1,0:T(8,128)(2,1)S(1)} fusion(bf16[512,128]{1,0:T(8,128)(2,1)} %param.6), kind=kLoop, calls=%fused_computation.42 | loop fusion | bytes 262144
  0.9 0.9 %constant_dynamic-update-slice_fusion.1 = bf16[512,384]{1,0:T(8,128)(2,1)S(1)} fusion(bf16[512,384]{1,0:T(8,128)(2,1)S(1)} %constant_dynamic-update-slice_fusion.2, bf16[512,128]{1,0:T(8,128)(2,1)} %param.7), kind=kLoop, calls=%fused_computation.41 | loop fusion | bytes 262144
  1.9 0.9 %constant_dynamic-update-slice_fusion = bf16[512,384]{1,0:T(8,128)(2,1)S(1)} fusion(bf16[512,384]{1,0:T(8,128)(2,1)S(1)} %constant_dynamic-update-slice_fusion.1, bf16[512,128]{1,0:T(8,128)(2,1)} %param.8), kind=kLoop, calls=%fused_computation.40 | loop fusion | bytes 262144 | tf_op jit(solution)/shard_map/concatenate | solution.py:59
  2.8 0.1 collective-permute-start
  2.9 0.1 collective-permute-start.1
  3.0 1.9 %collective-permute-start.3 = (bf16[512,384]{1,0:T(8,128)(2,1)S(1)}, bf16[512,384]{1,0:T(8,128)(2,1)}, u32[]{:S(2)}, u32[]{:S(2)}) collective-permute-start(bf16[512,384]{1,0:T(8,128)(2,1)S(1)} %constant_dynamic-update-slice_fusion), channel_id=1, source_target_pairs={{0,4},{1,5},{2,6},{3,7},{4,0},{5,1},{6,2},{7,3},{8,12},{9,13},{10,... | collective-permute-start | bytes 1179656 | tf_op jit(solution)/shard_map/ppermute | solution.py:39
  4.9 0.4 collective-permute-start.5
  5.3 1.5 %slice_bitcast_fusion = (bf16[96,4096]{1,0:T(8,128)(2,1)S(1)}, bf16[96,4096]{1,0:T(8,128)(2,1)S(1)}) fusion(bf16[1,192,4096]{2,1,0:T(8,128)(2,1)} %param.5), kind=kLoop, calls=%fused_computation.21 | loop fusion | bytes 3145728 | tf_op jit(solution)/shard_map/slice | solution.py:66
  6.8 0.0 copy-start
  6.8 1.6 %collective-permute-start.8 = (bf16[96,4096]{1,0:T(8,128)(2,1)S(1)}, bf16[96,4096]{1,0:T(8,128)(2,1)}, u32[]{:S(2)}, u32[]{:S(2)}) collective-permute-start(bf16[96,4096]{1,0:T(8,128)(2,1)S(1)} %get-tuple-element.6), channel_id=1, source_target_pairs={{0,16},{8,24},{16,0},{24,8},{1,17},{9,25},{17,1},{25,9},{2,18},{10... | collective-permute-start | bytes 2359304 | tf_op jit(solution)/shard_map/ppermute | solution.py:39
  8.4 0.1 constant_dynamic-slice_fusion.3
  8.5 0.1 pad_maximum_fusion.1
  8.6 0.1 pad_add_fusion
  8.7 0.3 broadcast_in_dim.50
  9.0 0.1 bitcast_dynamic-update-slice_fusion.7
  9.1 1.6 %collective-permute-start.7 = (bf16[192,4096]{1,0:T(8,128)(2,1)S(1)}, bf16[192,4096]{1,0:T(8,128)(2,1)S(1)}, u32[]{:S(2)}, u32[]{:S(2)}) collective-permute-start(bf16[192,4096]{1,0:T(8,128)(2,1)S(1)} %bitcast.51), channel_id=1, source_target_pairs={{0,8},{8,0},{16,24},{24,16},{1,9},{9,1},{17,25},{25,17},{2,10},{10... | collective-permute-start | bytes 4718600 | tf_op jit(solution)/shard_map/ppermute | solution.py:39
  10.6 4.1 %collective-permute-done.1 = bf16[512,384]{1,0:T(8,128)(2,1)} collective-permute-done((bf16[512,384]{1,0:T(8,128)(2,1)S(1)}, bf16[512,384]{1,0:T(8,128)(2,1)}, u32[]{:S(2)}, u32[]{:S(2)}) %collective-permute-start.1) | collective-permute-done | bytes 393248 | tf_op jit(solution)/shard_map/ppermute | solution.py:39
  14.7 1.1 %bitcast_dynamic-update-slice_fusion.6 = bf16[4,2,512,384]{3,2,1,0:T(8,128)(2,1)S(1)} fusion(bf16[4,2,512,384]{3,2,1,0:T(8,128)(2,1)S(1)} %bitcast_dynamic-update-slice_fusion.7, s32[]{:T(128)S(6)} %select_n.152, s32[]{:T(128)S(6)} %select_n.156, bf16[512,384]{1,0:T(8,128)(2,1)} %collective-permute-done), kind=kLoop, calls=%fused_computation.30 | loop fusion | bytes 786440 | tf_op jit(solution)/shard_map/dynamic_update_slice | solution.py:82
  15.8 1.1 %bitcast_dynamic-update-slice_fusion.5 = bf16[4,2,512,384]{3,2,1,0:T(8,128)(2,1)S(1)} fusion(bf16[4,2,512,384]{3,2,1,0:T(8,128)(2,1)S(1)} %bitcast_dynamic-update-slice_fusion.6, s32[]{:T(128)S(6)} %select_n.158, s32[]{:T(128)S(6)} %select_n.154, bf16[512,384]{1,0:T(8,128)(2,1)} %collective-permute-done.1), kind=kLoop, calls=%fused_computation.29 | loop fusion | bytes 786440 | tf_op jit(solution)/shard_map/dynamic_update_slice | solution.py:81
  16.8 22.9 %collective-permute-done.3 = bf16[512,384]{1,0:T(8,128)(2,1)} collective-permute-done((bf16[512,384]{1,0:T(8,128)(2,1)S(1)}, bf16[512,384]{1,0:T(8,128)(2,1)}, u32[]{:S(2)}, u32[]{:S(2)}) %collective-permute-start.3) | collective-permute-done | bytes 393248 | tf_op jit(solution)/shard_map/ppermute | solution.py:39
  39.7 1.5 %collective-permute-start.9 = (bf16[96,4096]{1,0:T(8,128)(2,1)S(1)}, bf16[96,4096]{1,0:T(8,128)(2,1)S(1)}, u32[]{:S(2)}, u32[]{:S(2)}) collective-permute-start(bf16[96,4096]{1,0:T(8,128)(2,1)S(1)} %get-tuple-element.5), channel_id=1, source_target_pairs={{0,16},{8,24},{16,0},{24,8},{1,17},{9,25},{17,1},{25,9},{2,18},{10... | collective-permute-start | bytes 2359304 | tf_op jit(solution)/shard_map/ppermute | solution.py:39
  41.2 0.5 collective-permute-start.6
  41.7 1.5 %collective-permute-start.10 = (bf16[96,4096]{1,0:T(8,128)(2,1)}, bf16[96,4096]{1,0:T(8,128)(2,1)S(1)}, u32[]{:S(2)}, u32[]{:S(2)}) collective-permute-start(bf16[96,4096]{1,0:T(8,128)(2,1)} %collective-permute-done.8), channel_id=1, source_target_pairs={{0,8},{8,0},{16,24},{24,16},{1,9},{9,1},{17,25},{25,17},{2,10},{10... | collective-permute-start | bytes 2359304 | tf_op jit(solution)/shard_map/ppermute | solution.py:39
  43.2 0.1 bitcast_dynamic-update-slice_fusion.4
  43.3 1.1 %bitcast_dynamic-update-slice_fusion.3 = bf16[4,2,512,384]{3,2,1,0:T(8,128)(2,1)S(1)} fusion(bf16[4,2,512,384]{3,2,1,0:T(8,128)(2,1)S(1)} %bitcast_dynamic-update-slice_fusion.4, s32[]{:T(128)S(6)} %select_n.160, s32[]{:T(128)S(6)} %select_n.154, bf16[512,384]{1,0:T(8,128)(2,1)} %collective-permute-done.3), kind=kLoop, calls=%fused_computation.27 | loop fusion | bytes 786440 | tf_op jit(solution)/shard_map/dynamic_update_slice | solution.py:81
  44.4 0.1 bitcast_dynamic-update-slice_fusion.2
  44.5 1.1 %bitcast_dynamic-update-slice_fusion.1 = bf16[4,2,512,384]{3,2,1,0:T(8,128)(2,1)S(1)} fusion(bf16[4,2,512,384]{3,2,1,0:T(8,128)(2,1)S(1)} %bitcast_dynamic-update-slice_fusion.2, s32[]{:T(128)S(6)} %select_n.162, s32[]{:T(128)S(6)} %select_n.154, bf16[512,384]{1,0:T(8,128)(2,1)} %collective-permute-done.5), kind=kLoop, calls=%fused_computation.25 | loop fusion | bytes 786440 | tf_op jit(solution)/shard_map/dynamic_update_slice | solution.py:81
  45.5 0.1 bitcast_dynamic-update-slice_fusion
  45.6 0.1 slice.48
  45.7 0.6 collective-permute-start.11
  46.3 13.8 %collective-permute-done.9 = bf16[96,4096]{1,0:T(8,128)(2,1)S(1)} collective-permute-done((bf16[96,4096]{1,0:T(8,128)(2,1)S(1)}, bf16[96,4096]{1,0:T(8,128)(2,1)S(1)}, u32[]{:S(2)}, u32[]{:S(2)}) %collective-permute-start.9) | collective-permute-done | bytes 786464 | tf_op jit(solution)/shard_map/ppermute | solution.py:39
  60.1 2.1 %fusion.18 = bf16[192,384]{1,0:T(8,128)(2,1)S(1)} fusion(bf16[4096,384]{1,0:T(8,128)(2,1)S(1)} %bitcast.47, bf16[96,4096]{1,0:T(8,128)(2,1)S(1)} %collective-permute-done.9, bf16[96,4096]{1,0:T(8,128)(2,1)} %collective-permute-done.8), kind=kOutput, calls=%fused_computation.16 | convolution fusion | flops 607199232 | bytes 4866048 | tf_op jit(solution)/shard_map/dot_general | solution.py:87
  62.2 1.0 %fusion.21 = bf16[192,384]{1,0:T(8,128)(2,1)S(1)} fusion(bf16[4096,384]{1,0:T(8,128)(2,1)S(1)} %bitcast.48, bf16[1,192,4096]{2,1,0:T(8,128)(2,1)S(1)} %copy-done), kind=kOutput, calls=%fused_computation.19 | convolution fusion | flops 604053504 | bytes 4866048 | tf_op jit(solution)/shard_map/dot_general | solution.py:87
  63.3 1.0 %fusion.22 = bf16[192,384]{1,0:T(8,128)(2,1)S(1)} fusion(bf16[192,4096]{1,0:T(8,128)(2,1)S(1)} %collective-permute-done.7, bf16[4096,384]{1,0:T(8,128)(2,1)S(1)} %bitcast.49), kind=kOutput, calls=%fused_computation.20 | convolution fusion | flops 604053504 | bytes 4866048 | tf_op jit(solution)/shard_map/dot_general | solution.py:87
  64.3 11.2 %collective-permute-done.11 = bf16[96,4096]{1,0:T(8,128)(2,1)S(1)} collective-permute-done((bf16[96,4096]{1,0:T(8,128)(2,1)S(1)}, bf16[96,4096]{1,0:T(8,128)(2,1)S(1)}, u32[]{:S(2)}, u32[]{:S(2)}) %collective-permute-start.11) | collective-permute-done | bytes 786464 | tf_op jit(solution)/shard_map/ppermute | solution.py:39
  75.6 1.0 %fusion.15 = bf16[192,384]{1,0:T(8,128)(2,1)S(1)} fusion(bf16[4096,384]{1,0:T(8,128)(2,1)S(1)} %bitcast.50, bf16[96,4096]{1,0:T(8,128)(2,1)S(1)} %collective-permute-done.11, bf16[96,4096]{1,0:T(8,128)(2,1)S(1)} %collective-permute-done.10), kind=kOutput, calls=%fused_computation.15 | convolution fusion | flops 607199232 | bytes 4866048 | tf_op jit(solution)/shard_map/dot_general | solution.py:87
  76.6 0.1 pad_maximum_fusion
  76.7 0.7 fusion.31
  77.3 0.4 fusion
  77.7 0.5 fusion.12
  78.3 2.5 %collective-permute-start.12 = (bf16[192,128]{1,0:T(8,128)(2,1)S(1)}, bf16[192,128]{1,0:T(8,128)(2,1)S(1)}, u32[]{:S(2)}, u32[]{:S(2)}) collective-permute-start(bf16[192,128]{1,0:T(8,128)(2,1)S(1)} %get-tuple-element.9), channel_id=1, source_target_pairs={{0,24},{8,16},{16,8},{24,0},{1,25},{9,17},{17,9},{25,1},{2,26},{10... | collective-permute-start | bytes 147464 | tf_op jit(solution)/shard_map/ppermute | solution.py:39
  80.8 0.5 collective-permute-start.13
  81.3 0.5 collective-permute-start.14
  81.8 1.5 %collective-permute-done.12 = bf16[192,128]{1,0:T(8,128)(2,1)S(1)} collective-permute-done((bf16[192,128]{1,0:T(8,128)(2,1)S(1)}, bf16[192,128]{1,0:T(8,128)(2,1)S(1)}, u32[]{:S(2)}, u32[]{:S(2)}) %collective-permute-start.12) | collective-permute-done | bytes 49184 | tf_op jit(solution)/shard_map/ppermute | solution.py:39
  83.4 1.5 %collective-permute-done.13 = bf16[192,128]{1,0:T(8,128)(2,1)S(1)} collective-permute-done((bf16[192,128]{1,0:T(8,128)(2,1)S(1)}, bf16[192,128]{1,0:T(8,128)(2,1)S(1)}, u32[]{:S(2)}, u32[]{:S(2)}) %collective-permute-start.13) | collective-permute-done | bytes 49184 | tf_op jit(solution)/shard_map/ppermute | solution.py:39
  84.9 0.5 collective-permute-done.14
  85.4 0.7 copy-done.1
  86.1 0.6 fusion.26
  (21 shorter events, 0.1 us)
Async XLA Ops:
  0.0 8.4 %copy-start.2 = (f32[1,1,768]{2,1,0:T(1,128)S(1)}, f32[1,1,768]{2,1,0:T(1,128)}, u32[]{:S(2)}) copy-start(f32[1,1,768]{2,1,0:T(1,128)} %param.9) | copy-start | bytes 9220
  2.8 6.2 %collective-permute-start = (bf16[512,384]{1,0:T(8,128)(2,1)S(1)}, bf16[512,384]{1,0:T(8,128)(2,1)}, u32[]{:S(2)}, u32[]{:S(2)}) collective-permute-start(bf16[512,384]{1,0:T(8,128)(2,1)S(1)} %constant_dynamic-update-slice_fusion), channel_id=1, source_target_pairs={{0,1},{1,0},{2,3},{3,2},{4,5},{5,4},{6,7},{7,6},{8,9},{9,8},{10,11... | collective-permute-start | bytes 1179656 | tf_op jit(solution)/shard_map/ppermute | solution.py:39
  2.9 11.8 %collective-permute-start.1 = (bf16[512,384]{1,0:T(8,128)(2,1)S(1)}, bf16[512,384]{1,0:T(8,128)(2,1)}, u32[]{:S(2)}, u32[]{:S(2)}) collective-permute-start(bf16[512,384]{1,0:T(8,128)(2,1)S(1)} %constant_dynamic-update-slice_fusion), channel_id=1, source_target_pairs={{0,2},{1,3},{2,4},{3,5},{4,6},{5,7},{6,0},{7,1},{8,10},{9,11},{10,... | collective-permute-start | bytes 1179656 | tf_op jit(solution)/shard_map/ppermute | solution.py:39
  3.0 36.7 %collective-permute-start.3 = (bf16[512,384]{1,0:T(8,128)(2,1)S(1)}, bf16[512,384]{1,0:T(8,128)(2,1)}, u32[]{:S(2)}, u32[]{:S(2)}) collective-permute-start(bf16[512,384]{1,0:T(8,128)(2,1)S(1)} %constant_dynamic-update-slice_fusion), channel_id=1, source_target_pairs={{0,4},{1,5},{2,6},{3,7},{4,0},{5,1},{6,2},{7,3},{8,12},{9,13},{10,... | collective-permute-start | bytes 1179656 | tf_op jit(solution)/shard_map/ppermute | solution.py:39
  4.9 36.3 %collective-permute-start.5 = (bf16[512,384]{1,0:T(8,128)(2,1)S(1)}, bf16[512,384]{1,0:T(8,128)(2,1)}, u32[]{:S(2)}, u32[]{:S(2)}) collective-permute-start(bf16[512,384]{1,0:T(8,128)(2,1)S(1)} %constant_dynamic-update-slice_fusion), channel_id=1, source_target_pairs={{0,6},{1,7},{2,0},{3,1},{4,2},{5,3},{6,4},{7,5},{8,14},{9,15},{10,... | collective-permute-start | bytes 1179656 | tf_op jit(solution)/shard_map/ppermute | solution.py:39
  6.8 2.3 %copy-start = (bf16[1,192,4096]{2,1,0:T(8,128)(2,1)S(1)}, bf16[1,192,4096]{2,1,0:T(8,128)(2,1)}, u32[]{:S(2)}) copy-start(bf16[1,192,4096]{2,1,0:T(8,128)(2,1)} %param.5) | copy-start | bytes 4718596
  6.8 34.9 %collective-permute-start.8 = (bf16[96,4096]{1,0:T(8,128)(2,1)S(1)}, bf16[96,4096]{1,0:T(8,128)(2,1)}, u32[]{:S(2)}, u32[]{:S(2)}) collective-permute-start(bf16[96,4096]{1,0:T(8,128)(2,1)S(1)} %get-tuple-element.6), channel_id=1, source_target_pairs={{0,16},{8,24},{16,0},{24,8},{1,17},{9,25},{17,1},{25,9},{2,18},{10... | collective-permute-start | bytes 2359304 | tf_op jit(solution)/shard_map/ppermute | solution.py:39
  9.1 36.5 %collective-permute-start.7 = (bf16[192,4096]{1,0:T(8,128)(2,1)S(1)}, bf16[192,4096]{1,0:T(8,128)(2,1)S(1)}, u32[]{:S(2)}, u32[]{:S(2)}) collective-permute-start(bf16[192,4096]{1,0:T(8,128)(2,1)S(1)} %bitcast.51), channel_id=1, source_target_pairs={{0,8},{8,0},{16,24},{24,16},{1,9},{9,1},{17,25},{25,17},{2,10},{10... | collective-permute-start | bytes 4718600 | tf_op jit(solution)/shard_map/ppermute | solution.py:39
  14.7 26.5 %collective-permute-start.2 = (bf16[512,384]{1,0:T(8,128)(2,1)}, bf16[512,384]{1,0:T(8,128)(2,1)S(1)}, u32[]{:S(2)}, u32[]{:S(2)}) collective-permute-start(bf16[512,384]{1,0:T(8,128)(2,1)} %collective-permute-done.1), channel_id=1, source_target_pairs={{0,1},{1,0},{2,3},{3,2},{4,5},{5,4},{6,7},{7,6},{8,9},{9,8},{10,11... | collective-permute-start | bytes 1179656 | tf_op jit(solution)/shard_map/ppermute | solution.py:39
  39.7 20.4 %collective-permute-start.9 = (bf16[96,4096]{1,0:T(8,128)(2,1)S(1)}, bf16[96,4096]{1,0:T(8,128)(2,1)S(1)}, u32[]{:S(2)}, u32[]{:S(2)}) collective-permute-start(bf16[96,4096]{1,0:T(8,128)(2,1)S(1)} %get-tuple-element.5), channel_id=1, source_target_pairs={{0,16},{8,24},{16,0},{24,8},{1,17},{9,25},{17,1},{25,9},{2,18},{10... | collective-permute-start | bytes 2359304 | tf_op jit(solution)/shard_map/ppermute | solution.py:39
  41.2 3.1 %collective-permute-start.4 = (bf16[512,384]{1,0:T(8,128)(2,1)}, bf16[512,384]{1,0:T(8,128)(2,1)S(1)}, u32[]{:S(2)}, u32[]{:S(2)}) collective-permute-start(bf16[512,384]{1,0:T(8,128)(2,1)} %collective-permute-done.3), channel_id=1, source_target_pairs={{0,1},{1,0},{2,3},{3,2},{4,5},{5,4},{6,7},{7,6},{8,9},{9,8},{10,11... | collective-permute-start | bytes 1179656 | tf_op jit(solution)/shard_map/ppermute | solution.py:39
  41.2 4.3 %collective-permute-start.6 = (bf16[512,384]{1,0:T(8,128)(2,1)}, bf16[512,384]{1,0:T(8,128)(2,1)S(1)}, u32[]{:S(2)}, u32[]{:S(2)}) collective-permute-start(bf16[512,384]{1,0:T(8,128)(2,1)} %collective-permute-done.5), channel_id=1, source_target_pairs={{0,1},{1,0},{2,3},{3,2},{4,5},{5,4},{6,7},{7,6},{8,9},{9,8},{10,11... | collective-permute-start | bytes 1179656 | tf_op jit(solution)/shard_map/ppermute | solution.py:39
  41.7 22.6 %collective-permute-start.10 = (bf16[96,4096]{1,0:T(8,128)(2,1)}, bf16[96,4096]{1,0:T(8,128)(2,1)S(1)}, u32[]{:S(2)}, u32[]{:S(2)}) collective-permute-start(bf16[96,4096]{1,0:T(8,128)(2,1)} %collective-permute-done.8), channel_id=1, source_target_pairs={{0,8},{8,0},{16,24},{24,16},{1,9},{9,1},{17,25},{25,17},{2,10},{10... | collective-permute-start | bytes 2359304 | tf_op jit(solution)/shard_map/ppermute | solution.py:39
  45.7 29.9 %collective-permute-start.11 = (bf16[96,4096]{1,0:T(8,128)(2,1)S(1)}, bf16[96,4096]{1,0:T(8,128)(2,1)S(1)}, u32[]{:S(2)}, u32[]{:S(2)}) collective-permute-start(bf16[96,4096]{1,0:T(8,128)(2,1)S(1)} %slice.48), channel_id=1, source_target_pairs={{0,16},{8,24},{16,0},{24,8},{1,17},{9,25},{17,1},{25,9},{2,18},{10... | collective-permute-start | bytes 2359304 | tf_op jit(solution)/shard_map/ppermute | solution.py:39
  78.3 5.1 %collective-permute-start.12 = (bf16[192,128]{1,0:T(8,128)(2,1)S(1)}, bf16[192,128]{1,0:T(8,128)(2,1)S(1)}, u32[]{:S(2)}, u32[]{:S(2)}) collective-permute-start(bf16[192,128]{1,0:T(8,128)(2,1)S(1)} %get-tuple-element.9), channel_id=1, source_target_pairs={{0,24},{8,16},{16,8},{24,0},{1,25},{9,17},{17,9},{25,1},{2,26},{10... | collective-permute-start | bytes 147464 | tf_op jit(solution)/shard_map/ppermute | solution.py:39
  80.8 4.1 %collective-permute-start.13 = (bf16[192,128]{1,0:T(8,128)(2,1)S(1)}, bf16[192,128]{1,0:T(8,128)(2,1)S(1)}, u32[]{:S(2)}, u32[]{:S(2)}) collective-permute-start(bf16[192,128]{1,0:T(8,128)(2,1)S(1)} %get-tuple-element.8), channel_id=1, source_target_pairs={{0,8},{8,0},{16,24},{24,16},{1,9},{9,1},{17,25},{25,17},{2,10},{10... | collective-permute-start | bytes 147464 | tf_op jit(solution)/shard_map/ppermute | solution.py:39
  81.3 4.1 %collective-permute-start.14 = (bf16[192,128]{1,0:T(8,128)(2,1)S(1)}, bf16[192,128]{1,0:T(8,128)(2,1)S(1)}, u32[]{:S(2)}, u32[]{:S(2)}) collective-permute-start(bf16[192,128]{1,0:T(8,128)(2,1)S(1)} %get-tuple-element.7), channel_id=1, source_target_pairs={{0,16},{8,24},{16,0},{24,8},{1,17},{9,25},{17,1},{25,9},{2,18},{10... | collective-permute-start | bytes 147464 | tf_op jit(solution)/shard_map/ppermute | solution.py:39
  85.4 0.7 copy-start.1

commit v4 on v3

--- a/solution.py
+++ b/solution.py
@@ -51,7 +51,7 @@
         width = query_weight.shape[1]
         own = tokens[0]
         rows = own.shape[0]
-        half = rows // 2
+        cut = rows // 2 + rows // 12
         s = lax.axis_index("sp")
         d = lax.axis_index("dp")
         y, x = s // side, s % side
@@ -62,8 +62,8 @@
         lower = {}
         for k in range(1, side):
             chunks[(0, k)] = send(own, "sp", sp, shift(0, k))
-            lower[k] = send(own[:half], "sp", sp, shift(k, 0))
-            upper = send(own[half:], "sp", sp, shift(k, 0))
+            lower[k] = send(own[:cut], "sp", sp, shift(k, 0))
+            upper = send(own[cut:], "sp", sp, shift(k, 0))
             chunks[(k, 0)] = jnp.concatenate([lower[k], upper], axis=0)
         stripes = [local]
         for k in range(1, planes):
@@ -71,7 +71,7 @@
         for j in range(1, side):
             for k in range(1, side):
                 first = send(lower[j], "sp", sp, shift(0, k))
-                second = send(chunks[(0, k)][half:], "sp", sp, shift(j, 0))
+                second = send(chunks[(0, k)][cut:], "sp", sp, shift(j, 0))
                 chunks[(j, k)] = jnp.concatenate([first, second], axis=0)
         whole = jnp.zeros((planes, cores) + local.shape, local.dtype)
         for k in range(planes):
@@ -94,14 +94,18 @@
         keys = projected[:, width : 2 * width]
         values = projected[:, 2 * width :]
         head_out = attend(queries, keys, values, jnp.concatenate(gates), jnp.concatenate(places))
+        received = {}
+        for n, (j, k) in sorted(enumerate(chunks), key=lambda entry: -sum(entry[1])):
+            part = head_out[n * rows : (n + 1) * rows]
+            received[j, k] = part if (j, k) == (0, 0) else send(part, "sp", sp, shift(-j, -k))
         gathered = jnp.zeros((rows, sp * width), head_out.dtype)
-        order = list(enumerate(chunks))
-        for n, (j, k) in sorted(order, key=lambda entry: -sum(entry[1])):
-            part = head_out[n * rows : (n + 1) * rows]
+        for (j, k), part in received.items():
+            if (j, k) == (0, 0):
+                gathered = lax.dynamic_update_slice(gathered, part, (0, s * width))
+        for (j, k), part in received.items():
             if (j, k) != (0, 0):
-                part = send(part, "sp", sp, shift(-j, -k))
-            head = (y + j) % side * side + (x + k) % side
-            gathered = lax.dynamic_update_slice(gathered, part, (0, head * width))
+                head = (y + j) % side * side + (x + k) % side
+                gathered = lax.dynamic_update_slice(gathered, part, (0, head * width))
         return gathered[None]
 
     return body

time: 87.1 us -> 81.1 us (0.931)
  waiting for transfers between devices: 55.6 us -> 47 us
  other arithmetic: 0.59 us -> 2.67 us
  local copies, waits for them, and re-layouts: 10.6 us -> 12.4 us
  matrix products: 6.4 us -> 5.1 us
    ppermute x15, waiting for transfers between devices: 55.6 us -> 47 us  [send(): return lax.ppermute(array, axis, [(i, target(i)) for i in range(count)])]
    slice x2 -> x3, local copies, waits for them, and re-layouts: 1.52 us -> 3.16 us  [the longest x1 2.21 us: body(): lower[k] = send(own[:cut], 'sp', sp, shift(k, 0))]
    dot_general x4, matrix products: 5.19 us -> 3.92 us  [body(): piece = jnp.dot(part, stacked, preferred_element_type=jnp.float32)]
    unnamed x8 -> x12, local copies, waits for them, and re-layouts: 2.56 us -> 2.16 us
  transfers between devices with their start and end apart: 15 -> 15, of which waited for: 7 -> 8; matrix products, arithmetic and copies ran while one was open for 12% -> 17% of each run, Pallas kernels for 0% -> 0%
where the time goes in v4:
time: 81.1 us; the launch traced here: 80.6 us
  waiting for transfers between devices  47 us (58%)
  starting transfers between devices  13.3 us (16%)
  local copies, waits for them, and re-layouts  12.4 us (15%)
  matrix products  5.1 us (6%)
  other arithmetic  2.67 us (3%)
    ppermute x15, waiting for transfers between devices, send(): return lax.ppermute(array, axis, [(i, target(i)) for i in range(count)])  47 us
    ppermute x15, starting transfers between devices, send(): return lax.ppermute(array, axis, [(i, target(i)) for i in range(count)])  13.3 us
    dot_general x4, matrix products, body(): piece = jnp.dot(part, stacked, preferred_element_type=jnp.float32)  3.92 us
    dynamic_update_slice x4, local copies, waits for them, and re-layouts, body(): lax.dynamic_update_slice(whole, stripe[None, None], (at, core, 0, 0))  3.26 us
    slice x1, local copies, waits for them, and re-layouts, body(): lower[k] = send(own[:cut], 'sp', sp, shift(k, 0))  2.21 us
    unnamed x12, local copies, waits for them, and re-layouts  2.16 us
  transfers between devices with their start and end apart: 15, of which 8 were waited for; matrix products, arithmetic and copies ran while one was open for 17% of the time, Pallas kernels for 0%

profile of v4, /device:TPU:24, one launch (start us, length us, event | category | flops | bytes accessed | tf_op | source)
XLA Modules:
  0.0 80.6 jit_solution(16208869785701456708)
XLA Ops:
  0.0 1.0 %constant_dynamic-update-slice_fusion.2 = bf16[512,384]{1,0:T(8,128)(2,1)S(1)} fusion(bf16[512,128]{1,0:T(8,128)(2,1)} %param.6), kind=kLoop, calls=%fused_computation.42 | loop fusion | bytes 262144
  1.1 0.9 %constant_dynamic-update-slice_fusion.1 = bf16[512,384]{1,0:T(8,128)(2,1)S(1)} fusion(bf16[512,384]{1,0:T(8,128)(2,1)S(1)} %constant_dynamic-update-slice_fusion.2, bf16[512,128]{1,0:T(8,128)(2,1)} %param.7), kind=kLoop, calls=%fused_computation.41 | loop fusion | bytes 262144
  2.0 0.9 %constant_dynamic-update-slice_fusion = bf16[512,384]{1,0:T(8,128)(2,1)S(1)} fusion(bf16[512,384]{1,0:T(8,128)(2,1)S(1)} %constant_dynamic-update-slice_fusion.1, bf16[512,128]{1,0:T(8,128)(2,1)} %param.8), kind=kLoop, calls=%fused_computation.40 | loop fusion | bytes 262144 | tf_op jit(solution)/shard_map/concatenate | solution.py:59
  2.9 0.1 collective-permute-start
  3.1 1.9 %collective-permute-start.3 = (bf16[512,384]{1,0:T(8,128)(2,1)S(1)}, bf16[512,384]{1,0:T(8,128)(2,1)}, u32[]{:S(2)}, u32[]{:S(2)}) collective-permute-start(bf16[512,384]{1,0:T(8,128)(2,1)S(1)} %constant_dynamic-update-slice_fusion), channel_id=1, source_target_pairs={{0,4},{1,5},{2,6},{3,7},{4,0},{5,1},{6,2},{7,3},{8,12},{9,13},{10,... | collective-permute-start | bytes 1179656 | tf_op jit(solution)/shard_map/ppermute | solution.py:39
  5.0 0.4 collective-permute-start.5
  5.4 1.5 %collective-permute-start.7 = (bf16[192,4096]{1,0:T(8,128)(2,1)}, bf16[192,4096]{1,0:T(8,128)(2,1)S(1)}, u32[]{:S(2)}, u32[]{:S(2)}) collective-permute-start(bf16[192,4096]{1,0:T(8,128)(2,1)} %bitcast.51), channel_id=1, source_target_pairs={{0,8},{8,0},{16,24},{24,16},{1,9},{9,1},{17,25},{25,17},{2,10},{10... | collective-permute-start | bytes 4718600 | tf_op jit(solution)/shard_map/ppermute | solution.py:39
  6.9 2.2 %slice_bitcast_fusion = bf16[112,4096]{1,0:T(8,128)(2,1)} fusion(bf16[1,192,4096]{2,1,0:T(8,128)(2,1)} %param.5), kind=kLoop, calls=%fused_computation.21 | loop fusion | bytes 1835008 | tf_op jit(solution)/shard_map/slice | solution.py:65
  9.1 0.9 %slice_bitcast_fusion.1 = bf16[80,4096]{1,0:T(8,128)(2,1)} fusion(bf16[1,192,4096]{2,1,0:T(8,128)(2,1)S(1)} %copy-done), kind=kLoop, calls=%fused_computation.22 | loop fusion | bytes 1310720 | tf_op jit(solution)/shard_map/slice | solution.py:66
  10.1 0.6 iota_add_fusion.2
  10.6 0.8 pad_add_fusion
  11.4 0.7 constant_dynamic-slice_fusion.3
  12.1 0.8 %pad_maximum_fusion.1 = f32[768]{0:T(1024)S(1)} fusion(f32[192]{0:T(256)} %bitcast.54, f32[192]{0:T(256)} %bitcast.55, f32[192]{0:T(256)S(1)} %bitcast.53, f32[192]{0:T(256)S(1)} %bitcast.52), kind=kLoop, calls=%fused_computation.44 | loop fusion | flops 2304 | bytes 6144 | tf_op jit(solution)/shard_map/concatenate | solution.py:96
  13.0 0.3 broadcast_in_dim.50
  13.2 0.1 bitcast_dynamic-update-slice_fusion.7
  13.3 1.6 %collective-permute-start.8 = (bf16[112,4096]{1,0:T(8,128)(2,1)S(1)}, bf16[112,4096]{1,0:T(8,128)(2,1)S(1)}, u32[]{:S(2)}, u32[]{:S(2)}) collective-permute-start(bf16[112,4096]{1,0:T(8,128)(2,1)S(1)} %copy-done.1), channel_id=1, source_target_pairs={{0,16},{8,24},{16,0},{24,8},{1,17},{9,25},{17,1},{25,9},{2,18},{10... | collective-permute-start | bytes 2752520 | tf_op jit(solution)/shard_map/ppermute | solution.py:39
  14.9 1.1 %bitcast_dynamic-update-slice_fusion.6 = bf16[4,2,512,384]{3,2,1,0:T(8,128)(2,1)S(1)} fusion(bf16[4,2,512,384]{3,2,1,0:T(8,128)(2,1)S(1)} %bitcast_dynamic-update-slice_fusion.7, s32[]{:T(128)S(6)} %select_n.148, s32[]{:T(128)S(6)} %select_n.152, bf16[512,384]{1,0:T(8,128)(2,1)} %collective-permute-done), kind=kLoop, calls=%fused_computation.30 | loop fusion | bytes 786440 | tf_op jit(solution)/shard_map/dynamic_update_slice | solution.py:82
  16.0 1.1 %bitcast_dynamic-update-slice_fusion.5 = bf16[4,2,512,384]{3,2,1,0:T(8,128)(2,1)S(1)} fusion(bf16[4,2,512,384]{3,2,1,0:T(8,128)(2,1)S(1)} %bitcast_dynamic-update-slice_fusion.6, s32[]{:T(128)S(6)} %select_n.154, s32[]{:T(128)S(6)} %select_n.150, bf16[512,384]{1,0:T(8,128)(2,1)} %collective-permute-done.1), kind=kLoop, calls=%fused_computation.29 | loop fusion | bytes 786440 | tf_op jit(solution)/shard_map/dynamic_update_slice | solution.py:81
  17.1 22.7 %collective-permute-done.3 = bf16[512,384]{1,0:T(8,128)(2,1)} collective-permute-done((bf16[512,384]{1,0:T(8,128)(2,1)S(1)}, bf16[512,384]{1,0:T(8,128)(2,1)}, u32[]{:S(2)}, u32[]{:S(2)}) %collective-permute-start.3) | collective-permute-done | bytes 393248 | tf_op jit(solution)/shard_map/ppermute | solution.py:39
  39.8 1.5 %collective-permute-start.9 = (bf16[80,4096]{1,0:T(8,128)(2,1)S(1)}, bf16[80,4096]{1,0:T(8,128)(2,1)S(1)}, u32[]{:S(2)}, u32[]{:S(2)}) collective-permute-start(bf16[80,4096]{1,0:T(8,128)(2,1)S(1)} %copy-done.2), channel_id=1, source_target_pairs={{0,16},{8,24},{16,0},{24,8},{1,17},{9,25},{17,1},{25,9},{2,18},{10... | collective-permute-start | bytes 1966088 | tf_op jit(solution)/shard_map/ppermute | solution.py:39
  41.3 0.5 collective-permute-start.6
  41.8 0.1 bitcast_dynamic-update-slice_fusion.4
  41.9 1.1 %bitcast_dynamic-update-slice_fusion.3 = bf16[4,2,512,384]{3,2,1,0:T(8,128)(2,1)S(1)} fusion(bf16[4,2,512,384]{3,2,1,0:T(8,128)(2,1)S(1)} %bitcast_dynamic-update-slice_fusion.4, s32[]{:T(128)S(6)} %select_n.156, s32[]{:T(128)S(6)} %select_n.150, bf16[512,384]{1,0:T(8,128)(2,1)} %collective-permute-done.3), kind=kLoop, calls=%fused_computation.27 | loop fusion | bytes 786440 | tf_op jit(solution)/shard_map/dynamic_update_slice | solution.py:81
  43.0 0.3 collective-permute-done.4
  43.3 0.1 bitcast_dynamic-update-slice_fusion.2
  43.3 1.1 %bitcast_dynamic-update-slice_fusion.1 = bf16[4,2,512,384]{3,2,1,0:T(8,128)(2,1)S(1)} fusion(bf16[4,2,512,384]{3,2,1,0:T(8,128)(2,1)S(1)} %bitcast_dynamic-update-slice_fusion.2, s32[]{:T(128)S(6)} %select_n.158, s32[]{:T(128)S(6)} %select_n.150, bf16[512,384]{1,0:T(8,128)(2,1)} %collective-permute-done.5), kind=kLoop, calls=%fused_computation.25 | loop fusion | bytes 786440 | tf_op jit(solution)/shard_map/dynamic_update_slice | solution.py:81
  44.4 0.1 bitcast_dynamic-update-slice_fusion
  44.5 1.6 %collective-permute-start.10 = (bf16[112,4096]{1,0:T(8,128)(2,1)S(1)}, bf16[112,4096]{1,0:T(8,128)(2,1)S(1)}, u32[]{:S(2)}, u32[]{:S(2)}) collective-permute-start(bf16[112,4096]{1,0:T(8,128)(2,1)S(1)} %collective-permute-done.8), channel_id=1, source_target_pairs={{0,8},{8,0},{16,24},{24,16},{1,9},{9,1},{17,25},{25,17},{2,10},{10... | collective-permute-start | bytes 2752520 | tf_op jit(solution)/shard_map/ppermute | solution.py:39
  46.1 1.0 %fusion.21 = bf16[192,384]{1,0:T(8,128)(2,1)S(1)} fusion(bf16[4096,384]{1,0:T(8,128)(2,1)S(1)} %bitcast.47, bf16[1,192,4096]{2,1,0:T(8,128)(2,1)S(1)} %copy-done), kind=kOutput, calls=%fused_computation.19 | convolution fusion | flops 604053504 | bytes 4866048 | tf_op jit(solution)/shard_map/dot_general | solution.py:87
  47.1 0.6 collective-permute-start.11
  47.7 9.7 %collective-permute-done.9 = bf16[80,4096]{1,0:T(8,128)(2,1)S(1)} collective-permute-done((bf16[80,4096]{1,0:T(8,128)(2,1)S(1)}, bf16[80,4096]{1,0:T(8,128)(2,1)S(1)}, u32[]{:S(2)}, u32[]{:S(2)}) %collective-permute-start.9) | collective-permute-done | bytes 655392 | tf_op jit(solution)/shard_map/ppermute | solution.py:39
  57.4 1.0 %fusion.18 = bf16[192,384]{1,0:T(8,128)(2,1)S(1)} fusion(bf16[4096,384]{1,0:T(8,128)(2,1)S(1)} %bitcast.48, bf16[80,4096]{1,0:T(8,128)(2,1)S(1)} %collective-permute-done.9, bf16[112,4096]{1,0:T(8,128)(2,1)S(1)} %collective-permute-done.8), kind=kOutput, calls=%fused_computation.16 | convolution fusion | flops 607199232 | bytes 4866048 | tf_op jit(solution)/shard_map/dot_general | solution.py:87
  58.4 1.0 %fusion.22 = bf16[192,384]{1,0:T(8,128)(2,1)S(1)} fusion(bf16[192,4096]{1,0:T(8,128)(2,1)S(1)} %collective-permute-done.7, bf16[4096,384]{1,0:T(8,128)(2,1)S(1)} %bitcast.49), kind=kOutput, calls=%fused_computation.20 | convolution fusion | flops 604053504 | bytes 4866048 | tf_op jit(solution)/shard_map/dot_general | solution.py:87
  59.4 7.6 %collective-permute-done.10 = bf16[112,4096]{1,0:T(8,128)(2,1)S(1)} collective-permute-done((bf16[112,4096]{1,0:T(8,128)(2,1)S(1)}, bf16[112,4096]{1,0:T(8,128)(2,1)S(1)}, u32[]{:S(2)}, u32[]{:S(2)}) %collective-permute-start.10) | collective-permute-done | bytes 917536 | tf_op jit(solution)/shard_map/ppermute | solution.py:39
  67.0 3.1 %collective-permute-done.11 = bf16[80,4096]{1,0:T(8,128)(2,1)S(1)} collective-permute-done((bf16[80,4096]{1,0:T(8,128)(2,1)S(1)}, bf16[80,4096]{1,0:T(8,128)(2,1)S(1)}, u32[]{:S(2)}, u32[]{:S(2)}) %collective-permute-start.11) | collective-permute-done | bytes 655392 | tf_op jit(solution)/shard_map/ppermute | solution.py:39
  70.1 1.0 %fusion.15 = bf16[192,384]{1,0:T(8,128)(2,1)S(1)} fusion(bf16[4096,384]{1,0:T(8,128)(2,1)S(1)} %bitcast.50, bf16[80,4096]{1,0:T(8,128)(2,1)S(1)} %collective-permute-done.11, bf16[112,4096]{1,0:T(8,128)(2,1)S(1)} %collective-permute-done.10), kind=kOutput, calls=%fused_computation.15 | convolution fusion | flops 607199232 | bytes 4866048 | tf_op jit(solution)/shard_map/dot_general | solution.py:87
  71.1 0.1 pad_maximum_fusion
  71.1 0.7 fusion.31
  71.8 0.4 fusion
  72.2 0.5 fusion.12
  72.7 2.5 %collective-permute-start.12 = (bf16[192,128]{1,0:T(8,128)(2,1)S(1)}, bf16[192,128]{1,0:T(8,128)(2,1)S(1)}, u32[]{:S(2)}, u32[]{:S(2)}) collective-permute-start(bf16[192,128]{1,0:T(8,128)(2,1)S(1)} %get-tuple-element.7), channel_id=1, source_target_pairs={{0,24},{8,16},{16,8},{24,0},{1,25},{9,17},{17,9},{25,1},{2,26},{10... | collective-permute-start | bytes 147464 | tf_op jit(solution)/shard_map/ppermute | solution.py:39
  75.2 0.5 collective-permute-start.13
  75.8 0.5 collective-permute-start.14
  76.3 1.5 %collective-permute-done.12 = bf16[192,128]{1,0:T(8,128)(2,1)S(1)} collective-permute-done((bf16[192,128]{1,0:T(8,128)(2,1)S(1)}, bf16[192,128]{1,0:T(8,128)(2,1)S(1)}, u32[]{:S(2)}, u32[]{:S(2)}) %collective-permute-start.12) | collective-permute-done | bytes 49184 | tf_op jit(solution)/shard_map/ppermute | solution.py:39
  77.8 1.5 %collective-permute-done.13 = bf16[192,128]{1,0:T(8,128)(2,1)S(1)} collective-permute-done((bf16[192,128]{1,0:T(8,128)(2,1)S(1)}, bf16[192,128]{1,0:T(8,128)(2,1)S(1)}, u32[]{:S(2)}, u32[]{:S(2)}) %collective-permute-start.13) | collective-permute-done | bytes 49184 | tf_op jit(solution)/shard_map/ppermute | solution.py:39
  79.4 0.5 collective-permute-done.14
  79.9 0.2 copy-done.3
  80.0 0.6 bitcast_dynamic-update-slice_fusion.8
  (26 shorter events, 0.2 us)
Async XLA Ops:
  0.0 9.1 %copy-start = (bf16[1,192,4096]{2,1,0:T(8,128)(2,1)S(1)}, bf16[1,192,4096]{2,1,0:T(8,128)(2,1)}, u32[]{:S(2)}) copy-start(bf16[1,192,4096]{2,1,0:T(8,128)(2,1)} %param.5) | copy-start | bytes 4718596
  0.0 11.4 %copy-start.4 = (f32[1,1,768]{2,1,0:T(1,128)S(1)}, f32[1,1,768]{2,1,0:T(1,128)}, u32[]{:S(2)}) copy-start(f32[1,1,768]{2,1,0:T(1,128)} %param.9) | copy-start | bytes 9220
  2.9 10.4 %collective-permute-start = (bf16[512,384]{1,0:T(8,128)(2,1)S(1)}, bf16[512,384]{1,0:T(8,128)(2,1)}, u32[]{:S(2)}, u32[]{:S(2)}) collective-permute-start(bf16[512,384]{1,0:T(8,128)(2,1)S(1)} %constant_dynamic-update-slice_fusion), channel_id=1, source_target_pairs={{0,1},{1,0},{2,3},{3,2},{4,5},{5,4},{6,7},{7,6},{8,9},{9,8},{10,11... | collective-permute-start | bytes 1179656 | tf_op jit(solution)/shard_map/ppermute | solution.py:39
  3.0 11.9 %collective-permute-start.1 = (bf16[512,384]{1,0:T(8,128)(2,1)S(1)}, bf16[512,384]{1,0:T(8,128)(2,1)}, u32[]{:S(2)}, u32[]{:S(2)}) collective-permute-start(bf16[512,384]{1,0:T(8,128)(2,1)S(1)} %constant_dynamic-update-slice_fusion), channel_id=1, source_target_pairs={{0,2},{1,3},{2,4},{3,5},{4,6},{5,7},{6,0},{7,1},{8,10},{9,11},{10,... | collective-permute-start | bytes 1179656 | tf_op jit(solution)/shard_map/ppermute | solution.py:39
  3.1 36.7 %collective-permute-start.3 = (bf16[512,384]{1,0:T(8,128)(2,1)S(1)}, bf16[512,384]{1,0:T(8,128)(2,1)}, u32[]{:S(2)}, u32[]{:S(2)}) collective-permute-start(bf16[512,384]{1,0:T(8,128)(2,1)S(1)} %constant_dynamic-update-slice_fusion), channel_id=1, source_target_pairs={{0,4},{1,5},{2,6},{3,7},{4,0},{5,1},{6,2},{7,3},{8,12},{9,13},{10,... | collective-permute-start | bytes 1179656 | tf_op jit(solution)/shard_map/ppermute | solution.py:39
  5.0 36.3 %collective-permute-start.5 = (bf16[512,384]{1,0:T(8,128)(2,1)S(1)}, bf16[512,384]{1,0:T(8,128)(2,1)}, u32[]{:S(2)}, u32[]{:S(2)}) collective-permute-start(bf16[512,384]{1,0:T(8,128)(2,1)S(1)} %constant_dynamic-update-slice_fusion), channel_id=1, source_target_pairs={{0,6},{1,7},{2,0},{3,1},{4,2},{5,3},{6,4},{7,5},{8,14},{9,15},{10,... | collective-permute-start | bytes 1179656 | tf_op jit(solution)/shard_map/ppermute | solution.py:39
  5.4 41.6 %collective-permute-start.7 = (bf16[192,4096]{1,0:T(8,128)(2,1)}, bf16[192,4096]{1,0:T(8,128)(2,1)S(1)}, u32[]{:S(2)}, u32[]{:S(2)}) collective-permute-start(bf16[192,4096]{1,0:T(8,128)(2,1)} %bitcast.51), channel_id=1, source_target_pairs={{0,8},{8,0},{16,24},{24,16},{1,9},{9,1},{17,25},{25,17},{2,10},{10... | collective-permute-start | bytes 4718600 | tf_op jit(solution)/shard_map/ppermute | solution.py:39
  12.1 1.2 %copy-start.1 = (bf16[112,4096]{1,0:T(8,128)(2,1)S(1)}, bf16[112,4096]{1,0:T(8,128)(2,1)}, u32[]{:S(2)}) copy-start(bf16[112,4096]{1,0:T(8,128)(2,1)} %slice_bitcast_fusion) | copy-start | bytes 2752516
  13.0 26.8 %copy-start.2 = (bf16[80,4096]{1,0:T(8,128)(2,1)S(1)}, bf16[80,4096]{1,0:T(8,128)(2,1)}, u32[]{:S(2)}) copy-start(bf16[80,4096]{1,0:T(8,128)(2,1)} %slice_bitcast_fusion.1) | copy-start | bytes 1966084
  13.3 31.2 %collective-permute-start.8 = (bf16[112,4096]{1,0:T(8,128)(2,1)S(1)}, bf16[112,4096]{1,0:T(8,128)(2,1)S(1)}, u32[]{:S(2)}, u32[]{:S(2)}) collective-permute-start(bf16[112,4096]{1,0:T(8,128)(2,1)S(1)} %copy-done.1), channel_id=1, source_target_pairs={{0,16},{8,24},{16,0},{24,8},{1,17},{9,25},{17,1},{25,9},{2,18},{10... | collective-permute-start | bytes 2752520 | tf_op jit(solution)/shard_map/ppermute | solution.py:39
  14.9 26.4 %collective-permute-start.2 = (bf16[512,384]{1,0:T(8,128)(2,1)}, bf16[512,384]{1,0:T(8,128)(2,1)S(1)}, u32[]{:S(2)}, u32[]{:S(2)}) collective-permute-start(bf16[512,384]{1,0:T(8,128)(2,1)} %collective-permute-done.1), channel_id=1, source_target_pairs={{0,1},{1,0},{2,3},{3,2},{4,5},{5,4},{6,7},{7,6},{8,9},{9,8},{10,11... | collective-permute-start | bytes 1179656 | tf_op jit(solution)/shard_map/ppermute | solution.py:39
  39.8 17.6 %collective-permute-start.9 = (bf16[80,4096]{1,0:T(8,128)(2,1)S(1)}, bf16[80,4096]{1,0:T(8,128)(2,1)S(1)}, u32[]{:S(2)}, u32[]{:S(2)}) collective-permute-start(bf16[80,4096]{1,0:T(8,128)(2,1)S(1)} %copy-done.2), channel_id=1, source_target_pairs={{0,16},{8,24},{16,0},{24,8},{1,17},{9,25},{17,1},{25,9},{2,18},{10... | collective-permute-start | bytes 1966088 | tf_op jit(solution)/shard_map/ppermute | solution.py:39
  41.3 1.9 %collective-permute-start.4 = (bf16[512,384]{1,0:T(8,128)(2,1)}, bf16[512,384]{1,0:T(8,128)(2,1)S(1)}, u32[]{:S(2)}, u32[]{:S(2)}) collective-permute-start(bf16[512,384]{1,0:T(8,128)(2,1)} %collective-permute-done.3), channel_id=1, source_target_pairs={{0,1},{1,0},{2,3},{3,2},{4,5},{5,4},{6,7},{7,6},{8,9},{9,8},{10,11... | collective-permute-start | bytes 1179656 | tf_op jit(solution)/shard_map/ppermute | solution.py:39
  41.3 3.1 %collective-permute-start.6 = (bf16[512,384]{1,0:T(8,128)(2,1)}, bf16[512,384]{1,0:T(8,128)(2,1)S(1)}, u32[]{:S(2)}, u32[]{:S(2)}) collective-permute-start(bf16[512,384]{1,0:T(8,128)(2,1)} %collective-permute-done.5), channel_id=1, source_target_pairs={{0,1},{1,0},{2,3},{3,2},{4,5},{5,4},{6,7},{7,6},{8,9},{9,8},{10,11... | collective-permute-start | bytes 1179656 | tf_op jit(solution)/shard_map/ppermute | solution.py:39
  44.5 22.5 %collective-permute-start.10 = (bf16[112,4096]{1,0:T(8,128)(2,1)S(1)}, bf16[112,4096]{1,0:T(8,128)(2,1)S(1)}, u32[]{:S(2)}, u32[]{:S(2)}) collective-permute-start(bf16[112,4096]{1,0:T(8,128)(2,1)S(1)} %collective-permute-done.8), channel_id=1, source_target_pairs={{0,8},{8,0},{16,24},{24,16},{1,9},{9,1},{17,25},{25,17},{2,10},{10... | collective-permute-start | bytes 2752520 | tf_op jit(solution)/shard_map/ppermute | solution.py:39
  47.1 23.0 %collective-permute-start.11 = (bf16[80,4096]{1,0:T(8,128)(2,1)S(1)}, bf16[80,4096]{1,0:T(8,128)(2,1)S(1)}, u32[]{:S(2)}, u32[]{:S(2)}) collective-permute-start(bf16[80,4096]{1,0:T(8,128)(2,1)S(1)} %slice.48), channel_id=1, source_target_pairs={{0,16},{8,24},{16,0},{24,8},{1,17},{9,25},{17,1},{25,9},{2,18},{10... | collective-permute-start | bytes 1966088 | tf_op jit(solution)/shard_map/ppermute | solution.py:39
  72.7 5.1 %collective-permute-start.12 = (bf16[192,128]{1,0:T(8,128)(2,1)S(1)}, bf16[192,128]{1,0:T(8,128)(2,1)S(1)}, u32[]{:S(2)}, u32[]{:S(2)}) collective-permute-start(bf16[192,128]{1,0:T(8,128)(2,1)S(1)} %get-tuple-element.7), channel_id=1, source_target_pairs={{0,24},{8,16},{16,8},{24,0},{1,25},{9,17},{17,9},{25,1},{2,26},{10... | collective-permute-start | bytes 147464 | tf_op jit(solution)/shard_map/ppermute | solution.py:39
  75.2 4.1 %collective-permute-start.13 = (bf16[192,128]{1,0:T(8,128)(2,1)S(1)}, bf16[192,128]{1,0:T(8,128)(2,1)S(1)}, u32[]{:S(2)}, u32[]{:S(2)}) collective-permute-start(bf16[192,128]{1,0:T(8,128)(2,1)S(1)} %get-tuple-element.6), channel_id=1, source_target_pairs={{0,8},{8,0},{16,24},{24,16},{1,9},{9,1},{17,25},{25,17},{2,10},{10... | collective-permute-start | bytes 147464 | tf_op jit(solution)/shard_map/ppermute | solution.py:39
  75.8 4.1 %collective-permute-start.14 = (bf16[192,128]{1,0:T(8,128)(2,1)S(1)}, bf16[192,128]{1,0:T(8,128)(2,1)S(1)}, u32[]{:S(2)}, u32[]{:S(2)}) collective-permute-start(bf16[192,128]{1,0:T(8,128)(2,1)S(1)} %get-tuple-element.5), channel_id=1, source_target_pairs={{0,16},{8,24},{16,0},{24,8},{1,17},{9,25},{17,1},{25,9},{2,18},{10... | collective-permute-start | bytes 147464 | tf_op jit(solution)/shard_map/ppermute | solution.py:39
  79.3 0.7 copy-start.3
